TPU v7x, 128 devices: a whole 4x4x4 slice. The times are simulated.
128 devices in a mesh: ep: 128 (over z, y, x, core).
Axes of the slice: x: 4, y: 4, z: 4, core: 2. Of those that a mesh axis runs over, the one named last changes fastest.
Arguments:
- tokens: bfloat16 [6144, 2048], P('ep'), may hold values from -6 to 6
- history_length: int32 [6144], P('ep'), may hold values from 1024 to 8192
- norm_gain: float32 [2048], replicated, may hold values from 0.1 to 1.9
- w_query: bfloat16 [2048, 512], replicated, may hold values from -0.125 to 0.125
- w_key: bfloat16 [2048, 512], replicated, may hold values from -0.125 to 0.125
- w_value: bfloat16 [2048, 512], replicated, may hold values from -0.125 to 0.125
- w_gate: bfloat16 [2048, 512], replicated, may hold values from -0.125 to 0.125
- decay_rate: float32 [8], replicated, may hold values from 0.003 to 0.7
- state: float32 [6144, 8, 64, 64], P('ep'), may hold values from -4 to 4
- head_gain: float32 [512], replicated, may hold values from 0.1 to 1.9
- w_out: bfloat16 [512, 2048], replicated, may hold values from -0.25 to 0.25
- moe_gain: float32 [2048], replicated, may hold values from 0.1 to 1.9
- route_weights: float32 [6144, 2], P('ep'), may hold values from 0.3 to 3
- expert_group: int32 [6144], P('ep'), may hold values from 0 to 3, as said below
- expert_inner: int32 [6144, 2], P('ep'), may hold values from 0 to 31, as said below
- expert_gate: bfloat16 [128, 2048, 256], P('ep'), may hold values from -0.125 to 0.125
- expert_up: bfloat16 [128, 2048, 256], P('ep'), may hold values from -0.125 to 0.125
- expert_down: bfloat16 [128, 256, 2048], P('ep'), may hold values from -0.375 to 0.375
Outputs:
- output: bfloat16 [6144, 2048], P('ep')
- new_state: float32 [6144, 8, 64, 64], P('ep')
Inputs may be any that keep to these rules, and one draw needn't show every extreme that they name: `expert_group`: together with expert_inner it names 2 different experts of one group for each token. `expert_inner`: the rows of one device name one expert at most 2 times; in every draw some expert is named exactly 2 times by the rows of every device.
All inputs are finite; a program needn't handle non-finite values.
Results may differ from a plain program's by a relative error of at most 0.02.
Values may be sent and summed in bfloat16 or wider, within the bound.
No kernel may reach another device: no remote copies, remote signals or barrier semaphores. Data moves between devices by JAX's collectives and lax.ppermute only.
A program may use at most 128 MiB of HBM per device.

v0:
```python
import jax
import jax.numpy as jnp
from jax import lax
from jax.sharding import PartitionSpec as P

GROUPS = 4
TOP_K = 2


epsilon = 1e-06


def rotate(values, places):
    halfway = values.shape[-1] // 2
    inverse = 10000.0 ** (-jnp.arange(halfway, dtype=jnp.float32) / halfway)
    angles = places[:, None] * inverse[None, :]
    cosine = jnp.cos(angles)[:, None, :]
    sine_table = jnp.sin(angles)[:, None, :]
    first_half = values[..., :halfway]
    second = values[..., halfway:]
    return jnp.concatenate(
        [first_half * cosine - second * sine_table, first_half * sine_table + second * cosine],
        axis=-1,
    )


def rms_scale(values, gains):
    return values * lax.rsqrt(jnp.mean(values * values, axis=-1, keepdims=True) + epsilon) * gains


def retention_step(
    tokens,
    history_length,
    norm_gain,
    w_query,
    w_key,
    w_value,
    w_gate,
    decay_rate,
    state,
    head_gain,
    w_out,
    moe_gain,
):
    row_count = tokens.shape[0]
    head_count = decay_rate.shape[0]
    head_width = state.shape[-1]
    inputs = tokens.astype(jnp.float32)
    normed = rms_scale(inputs, norm_gain).astype(jnp.bfloat16)

    def project(weights):
        return jnp.dot(normed, weights, preferred_element_type=jnp.float32).astype(jnp.bfloat16)

    queries = project(w_query).reshape(row_count, head_count, head_width).astype(jnp.float32)
    keys_now = project(w_key).reshape(row_count, head_count, head_width).astype(jnp.float32)
    values_now = project(w_value).reshape(row_count, head_count, head_width).astype(jnp.float32)
    gating = project(w_gate).astype(jnp.float32)
    places = history_length.astype(jnp.float32)
    queries = rotate(queries, places)
    keys_now = rotate(keys_now, places) * head_width ** (-0.5)
    retain = jnp.exp(-decay_rate)
    new_state = (
        retain[None, :, None, None] * state + keys_now[:, :, :, None] * values_now[:, :, None, :]
    )
    reading = jnp.einsum("bhk,bhkv->bhv", queries, new_state)
    reading = rms_scale(reading, head_gain.reshape(head_count, head_width))
    mixed_heads = (
        reading.reshape(row_count, head_count * head_width) * jax.nn.silu(gating)
    ).astype(jnp.bfloat16)
    mixed_tokens = (
        inputs + jnp.dot(mixed_heads, w_out, preferred_element_type=jnp.float32)
    ).astype(jnp.bfloat16)
    normed_moe = rms_scale(mixed_tokens.astype(jnp.float32), moe_gain).astype(jnp.bfloat16)
    return (mixed_tokens, normed_moe, new_state)


def expert_apply(row_block, gate_weight, up_weight, down_weight):
    gate_part = jnp.dot(row_block, gate_weight, preferred_element_type=jnp.float32)
    up_part = jnp.dot(row_block, up_weight, preferred_element_type=jnp.float32)
    hidden = (jax.nn.silu(gate_part) * up_part).astype(jnp.bfloat16)
    return jnp.dot(hidden, down_weight, preferred_element_type=jnp.float32).astype(jnp.bfloat16)


def slot_positions(flat_ids, experts):
    onehot = (flat_ids[:, None] == jnp.arange(experts, dtype=jnp.int32)[None, :]).astype(jnp.int32)
    earlier = jnp.cumsum(onehot, axis=0) - onehot
    return jnp.sum(earlier * onehot, axis=1)


def local(
    tokens,
    history_length,
    norm_gain,
    w_query,
    w_key,
    w_value,
    w_gate,
    decay_rate,
    state,
    head_gain,
    w_out,
    moe_gain,
    route_weights,
    expert_group,
    expert_inner,
    expert_gate,
    expert_up,
    expert_down,
):
    experts = lax.axis_size("ep")
    per_group = experts // GROUPS
    seq_count = tokens.shape[0]
    capacity = max(2, 4 * seq_count // experts)
    model_width = tokens.shape[1]
    expert_ids = expert_group[:, None] * per_group + expert_inner
    mixed_tokens, normed_moe, new_state = retention_step(
        tokens,
        history_length,
        norm_gain,
        w_query,
        w_key,
        w_value,
        w_gate,
        decay_rate,
        state,
        head_gain,
        w_out,
        moe_gain,
    )
    flat_ids = expert_ids.reshape(-1)
    target = flat_ids * capacity + slot_positions(flat_ids, experts)
    placement_table = (
        target[:, None] == jnp.arange(experts * capacity, dtype=jnp.int32)[None, :]
    ).astype(jnp.bfloat16)
    repeated = jnp.repeat(normed_moe, TOP_K, axis=0)
    outgoing = jnp.einsum(
        "rs,rd->sd", placement_table, repeated, preferred_element_type=jnp.float32
    )
    outgoing = outgoing.astype(jnp.bfloat16).reshape(experts, capacity, model_width)
    incoming = lax.all_to_all(outgoing, "ep", split_axis=0, concat_axis=0, tiled=True)
    flat_rows = incoming.reshape(-1, model_width)
    outputs = expert_apply(flat_rows, expert_gate[0], expert_up[0], expert_down[0]).reshape(
        incoming.shape
    )
    returned_rows = lax.all_to_all(outputs, "ep", split_axis=0, concat_axis=0, tiled=True)
    collected = jnp.einsum(
        "rs,sd->rd",
        placement_table,
        returned_rows.reshape(experts * capacity, model_width),
        preferred_element_type=jnp.float32,
    )
    collected = collected.reshape(-1, TOP_K, model_width)
    routed = jnp.sum(collected * route_weights[:, :, None], axis=1)
    output = (mixed_tokens.astype(jnp.float32) + routed).astype(jnp.bfloat16)
    return (output, new_state)


def solution(mesh):
    return jax.shard_map(
        local,
        mesh=mesh,
        in_specs=(
            P("ep", None),
            P("ep"),
            P(),
            P(),
            P(),
            P(),
            P(),
            P(),
            P("ep", None, None, None),
            P(),
            P(),
            P(),
            P("ep", None),
            P("ep"),
            P("ep", None),
            P("ep", None, None),
            P("ep", None, None),
            P("ep", None, None),
        ),
        out_specs=(P("ep", None), P("ep", None, None, None)),
        check_vma=False,
    )
```

profile of v0, /device:TPU:1, one launch (start us, length us, event | category | flops | bytes accessed | tf_op | source)
XLA Modules:
  0.0 104.1 jit_solution(1224752899276910808)
XLA Ops:
  0.6 0.0 copy-start
  0.6 0.0 copy-start.2
  0.7 0.0 copy-start.4
  0.7 0.8 broadcast_multiply_fusion
  1.5 0.7 convert_element_type.80
  2.2 0.7 negate_exponential_fusion
  2.8 1.1 %fusion.13 = f32[48]{0:T(128)S(1)} fusion(bf16[48,2048]{1,0:T(8,128)(2,1)} %param.18), kind=kLoop, calls=%fused_computation.24 | loop fusion | flops 294864 | bytes 196800 | tf_op jit(solution)/shard_map/reduce_sum | solution.py:28
  3.9 0.8 mul.244
  4.7 0.7 broadcast_add_fusion
  5.3 0.1 copy.29
  5.4 0.1 eq.50
  5.6 0.1 fusion.26
  5.7 0.1 reduce_window_sum.11
  5.8 0.2 select_reduce_fusion
  6.0 2.2 %fusion.6 = f32[48,512]{1,0:T(8,128)S(1)} fusion(bf16[2048,512]{1,0:T(8,128)(2,1)} %param.22, bf16[48,2048]{1,0:T(8,128)(2,1)} %param.18, f32[2048]{0:T(1024)} %param.20, f32[48]{0:T(128)S(1)} %add_rsqrt_fusion.2), kind=kOutput, calls=%fused_computation.15 | convolution fusion | flops 101105664 | bytes 2400448 | tf_op jit(solution)/shard_map/dot_general | solution.py:52
  8.2 0.1 reshape.175
  8.3 0.0 copy-done.2
  8.3 0.0 copy-done.4
  8.3 2.1 %fusion.5 = f32[48,512]{1,0:T(8,128)S(1)} fusion(bf16[2048,512]{1,0:T(8,128)(2,1)} %param.23, bf16[48,2048]{1,0:T(8,128)(2,1)S(1)} %copy-done.2, f32[2048]{0:T(1024)S(1)} %copy-done.4, f32[48]{0:T(128)S(1)} %add_rsqrt_fusion.2), kind=kOutput, calls=%fused_computation.13 | convolution fusion | flops 101105664 | bytes 2400448 | tf_op jit(solution)/shard_map/dot_general | solution.py:52
  10.5 0.1 reshape.176
  10.5 2.1 %fusion.7 = f32[48,512]{1,0:T(8,128)S(1)} fusion(bf16[2048,512]{1,0:T(8,128)(2,1)} %param.21, bf16[48,2048]{1,0:T(8,128)(2,1)S(1)} %copy-done.2, f32[2048]{0:T(1024)S(1)} %copy-done.4, f32[48]{0:T(128)S(1)} %add_rsqrt_fusion.2), kind=kOutput, calls=%fused_computation.17 | convolution fusion | flops 101105664 | bytes 2400448 | tf_op jit(solution)/shard_map/dot_general | solution.py:52
  12.7 0.1 reshape.174
  12.8 0.2 multiply_cosine_fusion
  12.9 0.2 multiply_subtract_fusion
  13.2 0.2 pad_maximum_fusion
  13.3 8.5 %multiply_add_fusion = f32[48,8,64,64]{3,2,1,0:T(8,128)S(1)} fusion(f32[48,8,64,64]{3,2,1,0:T(8,128)} %param.26, f32[48,8,64]{2,1,0:T(8,128)S(1)} %reshape.176, f32[48,8,64]{2,1,0:T(8,128)S(1)} %get-tuple-element.13, f32[8]{0:T(128)S(1)} %negate_exponential_fusion), kind=kLoop, calls=%fused_computation | loop fusion | flops 4718592 | bytes 12779552 | tf_op jit(solution)/shard_map/add | solution.py:63
  21.8 0.0 copy-start.1
  21.8 1.8 %fusion.37 = f32[48,8,1,64]{3,2,1,0:T(1,128)S(1)} fusion(f32[48,8,64,1]{2,3,1,0:T(1,128)S(1)} %bitcast.31, f32[48,8,64,64]{3,2,1,0:T(8,128)S(1)} %multiply_add_fusion), kind=kOutput, calls=%fused_computation.67 | convolution fusion | flops 3145728 | bytes 6488064 | tf_op jit(solution)/shard_map/bhk,bhkv->bhv/dot_general | solution.py:65
  23.6 3.0 %copy-done.1 = f32[48,8,64,64]{3,2,1,0:T(8,128)} copy-done((f32[48,8,64,64]{3,2,1,0:T(8,128)}, f32[48,8,64,64]{3,2,1,0:T(8,128)S(1)}, u32[]{:S(2)}) %copy-start.1) | copy-done | bytes 6291480
  26.6 0.1 multiply_reduce_fusion.1
  26.7 0.1 copy.27
  26.8 0.1 copy.28
  26.9 0.1 multiply_multiply_fusion
  27.0 0.1 reshape.168
  27.1 0.0 copy-done
  27.1 0.0 copy-start.5
  27.1 2.7 %multiply_reduce_fusion = (f32[48]{0:T(128)S(1)}, f32[48,2048]{1,0:T(8,128)S(1)}) fusion(bf16[512,2048]{1,0:T(8,128)(2,1)S(1)} %copy-done, f32[48,512]{1,0:T(8,128)S(1)} %reshape.168, bf16[2048,512]{1,0:T(8,128)(2,1)} %param.24, bf16[48,2048]{1,0:T(8,128)(2,1)S(1)} %copy-done.2, f32[2048]{0:T(1024)S(1)} %copy-done.4, f32[48]{0:T(128)S(1)} %add_rsqrt_fusion.2), kind=kOutput, calls=%fused_computation.29 | convolution fusion | flops 202506192 | bytes 4891008 | tf_op jit(solution)/shard_map/dot_general | solution.py:71
  29.8 0.0 copy-start.3
  29.8 0.0 copy-done.5
  29.8 0.1 multiply_convert_fusion
  30.0 0.2 broadcast_in_dim.2
  30.2 0.4 copy-done.3
  30.6 0.9 reshape.169
  31.5 1.5 %convolution_convert_fusion = bf16[256,2048]{1,0:T(8,128)(2,1)S(1)} fusion(bf16[96,2048]{1,0:T(8,128)(2,1)} %reshape.169, s32[96]{0:T(128)S(1)} %multiply_add_fusion.4), kind=kOutput, calls=%fused_computation.1 | convolution fusion | flops 101212160 | bytes 1442176 | tf_op jit(solution)/shard_map/rs,rd->sd/dot_general | solution.py:136
  33.0 1.5 %reshape.170 = bf16[128,2,2048]{2,1,0:T(2,128)(2,1)} reshape(bf16[256,2048]{1,0:T(8,128)(2,1)S(1)} %convolution_convert_fusion) | data formatting | bytes 2097152 | tf_op jit(solution)/shard_map/reshape | solution.py:139
  34.5 30.8 %all_to_all.10 = bf16[128,2,2048]{2,1,0:T(2,128)(2,1)} all-to-all(bf16[128,2,2048]{2,1,0:T(2,128)(2,1)} %reshape.170), channel_id=1, replica_groups=mesh['ep'=128] {'ep'}, dimensions={0} | all-to-all | bytes 2097152 | tf_op jit(solution)/shard_map/all_to_all | solution.py:140
  65.4 1.5 %reshape.171 = bf16[256,2048]{1,0:T(8,128)(2,1)S(1)} reshape(bf16[128,2,2048]{2,1,0:T(2,128)(2,1)} %all_to_all.10) | data formatting | bytes 2097152 | tf_op jit(solution)/shard_map/reshape | solution.py:141
  66.8 2.4 %fusion.11 = f32[256,256]{1,0:T(8,128)} fusion(bf16[256,2048]{1,0:T(8,128)(2,1)S(1)} %reshape.171, bf16[1,2048,256]{2,1,0:T(8,128)(2,1)} %param.33), kind=kOutput, calls=%fused_computation.20 | convolution fusion | flops 268435456 | bytes 2359296 | tf_op jit(solution)/shard_map/dot_general | solution.py:78
  69.2 3.9 %convolution_convert_fusion.1 = bf16[256,2048]{1,0:T(8,128)(2,1)} fusion(bf16[256,2048]{1,0:T(8,128)(2,1)S(1)} %reshape.171, bf16[1,256,2048]{2,1,0:T(8,128)(2,1)} %param.35, bf16[1,2048,256]{2,1,0:T(8,128)(2,1)} %param.34, f32[256,256]{1,0:T(8,128)} %fusion.11), kind=kOutput, calls=%fused_computation.2 | convolution fusion | flops 537788416 | bytes 4456448 | tf_op jit(solution)/shard_map/dot_general | solution.py:81
  73.1 0.0 copy-start.6
  73.1 2.6 %reshape.172 = bf16[128,2,2048]{2,1,0:T(2,128)(2,1)} reshape(bf16[256,2048]{1,0:T(8,128)(2,1)} %convolution_convert_fusion.1) | data formatting | bytes 2097152 | tf_op jit(solution)/shard_map/reshape | solution.py:142
  75.7 0.0 copy-start.7
  75.7 4.5 %all-to-all-start.1 = ((bf16[128,2,2048]{2,1,0:T(2,128)(2,1)}), bf16[128,2,2048]{2,1,0:T(2,128)(2,1)S(1)}, u32[]{:S(2)}, u32[]{:S(2)}) async-start(bf16[128,2,2048]{2,1,0:T(2,128)(2,1)} %reshape.172), calls=%async_computation.1 | async-start | bytes 2097152 | tf_op jit(solution)/shard_map/all_to_all | solution.py:145
  80.2 0.1 reduce_sum.50
  80.3 0.1 copy.30
  80.4 0.0 copy-done.6
  80.4 19.2 %all-to-all-done.1 = bf16[128,2,2048]{2,1,0:T(2,128)(2,1)S(1)} async-done(((bf16[128,2,2048]{2,1,0:T(2,128)(2,1)}), bf16[128,2,2048]{2,1,0:T(2,128)(2,1)S(1)}, u32[]{:S(2)}, u32[]{:S(2)}) %all-to-all-start.1) | async-done | bytes 1048608 | tf_op jit(solution)/shard_map/all_to_all | solution.py:145
  99.6 1.2 %reshape.179 = bf16[256,2048,1]{1,0,2:T(8,128)(2,1)} reshape(bf16[128,2,2048]{2,1,0:T(2,128)(2,1)S(1)} %all-to-all-done.1) | data formatting | bytes 2097152 | tf_op jit(solution)/shard_map/reshape | solution.py:149
  100.8 0.0 copy-done.7
  100.8 1.6 %fusion.2 = f32[48,2048]{1,0:T(8,128)S(1)} fusion(bf16[256,2048,1]{1,0,2:T(8,128)(2,1)} %reshape.179, f32[48,2]{0,1:T(2,128)S(1)} %copy-done.7, s32[48,2]{0,1:T(2,128)S(1)} %multiply_add_fusion.3), kind=kOutput, calls=%fused_computation.7 | convolution fusion | flops 100982784 | bytes 1442560 | tf_op jit(solution)/shard_map/rs,sd->rd/dot_general | solution.py:146
  102.4 1.7 %add_convert_fusion = bf16[48,2048]{1,0:T(8,128)(2,1)} fusion(f32[48,2048]{1,0:T(8,128)} %copy-done.3, f32[48,2048]{1,0:T(8,128)S(1)} %fusion.2), kind=kLoop, calls=%fused_computation.27 | loop fusion | flops 196608 | bytes 983040 | tf_op jit(solution)/shard_map/convert_element_type | solution.py:154
  (6 shorter events, 0.0 us)
Async XLA Ops:
  0.6 26.5 %copy-start = (bf16[512,2048]{1,0:T(8,128)(2,1)S(1)}, bf16[512,2048]{1,0:T(8,128)(2,1)}, u32[]{:S(2)}) copy-start(bf16[512,2048]{1,0:T(8,128)(2,1)} %param.28) | copy-start | bytes 6291460
  0.6 7.7 %copy-start.2 = (bf16[48,2048]{1,0:T(8,128)(2,1)S(1)}, bf16[48,2048]{1,0:T(8,128)(2,1)}, u32[]{:S(2)}) copy-start(bf16[48,2048]{1,0:T(8,128)(2,1)} %param.18) | copy-start | bytes 589828
  0.7 7.7 %copy-start.4 = (f32[2048]{0:T(1024)S(1)}, f32[2048]{0:T(1024)}, u32[]{:S(2)}) copy-start(f32[2048]{0:T(1024)} %param.20) | copy-start | bytes 24580
  21.8 4.8 %copy-start.1 = (f32[48,8,64,64]{3,2,1,0:T(8,128)}, f32[48,8,64,64]{3,2,1,0:T(8,128)S(1)}, u32[]{:S(2)}) copy-start(f32[48,8,64,64]{3,2,1,0:T(8,128)S(1)} %multiply_add_fusion) | copy-start | bytes 18874372
  27.1 2.7 %copy-start.5 = (f32[2048]{0:T(1024)S(1)}, f32[2048]{0:T(1024)}, u32[]{:S(2)}) copy-start(f32[2048]{0:T(1024)} %param.29) | copy-start | bytes 24580
  29.8 0.8 copy-start.3
  73.1 7.3 %copy-start.6 = (s32[48,2]{0,1:T(2,128)S(1)}, s32[48,2]{0,1:T(2,128)}, u32[]{:S(2)}) copy-start(s32[48,2]{0,1:T(2,128)} %param.32) | copy-start | bytes 1156
  75.7 25.1 %copy-start.7 = (f32[48,2]{0,1:T(2,128)S(1)}, f32[48,2]{0,1:T(2,128)}, u32[]{:S(2)}) copy-start(f32[48,2]{0,1:T(2,128)} %param.30) | copy-start | bytes 1156
  75.7 23.9 %all-to-all-start.1 = ((bf16[128,2,2048]{2,1,0:T(2,128)(2,1)}), bf16[128,2,2048]{2,1,0:T(2,128)(2,1)S(1)}, u32[]{:S(2)}, u32[]{:S(2)}) async-start(bf16[128,2,2048]{2,1,0:T(2,128)(2,1)} %reshape.172), calls=%async_computation.1 | async-start | bytes 2097152 | tf_op jit(solution)/shard_map/all_to_all | solution.py:145
where the time goes:
time: 105 us; the launch traced here: 104 us
  blocking collectives  30.8 us (29%)
  matrix products  20.3 us (19%)
  waiting for transfers between devices  19.2 us (18%)
  other arithmetic  15.4 us (15%)
  local copies, waits for them, and re-layouts  13 us (12%)
  starting transfers between devices  4.52 us (4%)
    all_to_all x1, blocking collectives, local(): lax.all_to_all(outgoing, 'ep', split_axis=0, concat_axis=0, tiled=True)  30.8 us
    all_to_all x1, waiting for transfers between devices, local(): lax.all_to_all(outputs, 'ep', split_axis=0, concat_axis=0, tiled=True)  19.2 us
    add x1, other arithmetic, retention_step(): retain[None, :, None, None] * state  8.48 us
    dot_general x3, matrix products, project(): jnp.dot(normed, weights, preferred_element_type=jnp.float32)  6.44 us
    all_to_all x1, starting transfers between devices, local(): lax.all_to_all(outputs, 'ep', split_axis=0, concat_axis=0, tiled=True)  4.52 us
    dot_general x1, matrix products, expert_apply(): jnp.dot(hidden, down_weight, preferred_element_type=jnp.float32)  3.91 us
    unnamed x16, local copies, waits for them, and re-layouts  3.43 us
    dot_general x1, matrix products, retention_step(): jnp.dot(mixed_heads, w_out, preferred_element_type=jnp.float32)  2.67 us
  transfers between devices with their start and end apart: 1, of which 1 were waited for; matrix products, arithmetic and copies ran while one was open for 0% of the time, Pallas kernels for 0%

commit v1 on v0

v1 whole, which is shorter than its diff:
```python
import functools

import jax
import jax.numpy as jnp
import numpy as np
from jax import lax
from jax.experimental import pallas as pl
from jax.experimental.pallas import tpu as pltpu
from jax.sharding import PartitionSpec as P

EPS = 1e-06
ROWS = 48
D = 2048
HEADS = 8
HD = 64
RW = HEADS * HD
EXPERTS = 128
PER_GROUP = 32
LANES = 128
TILES = D // LANES
GROUP = 8
CHUNKS = ROWS // GROUP
F32 = jnp.float32
BF16 = jnp.bfloat16


def lane_iota(shape):
    return lax.broadcasted_iota(jnp.int32, shape, len(shape) - 1)


def group_sum(x, ones):
    high = x.astype(BF16)
    low = (x - high.astype(F32)).astype(BF16)
    return jnp.dot(high, ones, preferred_element_type=F32) + jnp.dot(
        low, ones, preferred_element_type=F32
    )


def rope(x, cosine, sine):
    lanes = lane_iota((ROWS, LANES))
    first = (lanes % HD) < (HD // 2)
    parts = []
    for c in range(RW // LANES):
        part = x[:, c * LANES : (c + 1) * LANES]
        other = jnp.where(
            first,
            pltpu.roll(part, LANES - HD // 2, 1),
            pltpu.roll(part, HD // 2, 1),
        )
        parts.append(part * cosine + other * jnp.where(first, -sine, sine))
    return jnp.concatenate(parts, axis=1)


def front_kernel(
    hist_hbm,
    inv_hbm,
    ngain_hbm,
    decay_hbm,
    hgain_hbm,
    mgain_hbm,
    group_hbm,
    inner_hbm,
    tok_hbm,
    wq_hbm,
    wk_hbm,
    wv_hbm,
    wg_hbm,
    state_hbm,
    wo_hbm,
    mixed_ref,
    send0_ref,
    send1_ref,
    k_ref,
    v_ref,
    hist,
    inv,
    ngain,
    decay,
    hgain,
    mgain,
    group,
    inner,
    tok,
    w4,
    wo,
    st,
    qs,
    part,
    wide,
    tiles,
    small_sem,
    w_sem,
    st_sem,
):
    small = [
        pltpu.make_async_copy(tok_hbm, tok, small_sem.at[0]),
        pltpu.make_async_copy(ngain_hbm, ngain, small_sem.at[1]),
        pltpu.make_async_copy(hist_hbm, hist, small_sem.at[2]),
        pltpu.make_async_copy(inv_hbm, inv, small_sem.at[3]),
        pltpu.make_async_copy(decay_hbm, decay, small_sem.at[4]),
        pltpu.make_async_copy(hgain_hbm, hgain, small_sem.at[5]),
        pltpu.make_async_copy(mgain_hbm, mgain, small_sem.at[6]),
        pltpu.make_async_copy(group_hbm, group, small_sem.at[7]),
        pltpu.make_async_copy(inner_hbm, inner, small_sem.at[8]),
    ]
    for copy in small:
        copy.start()
    weights = [
        pltpu.make_async_copy(src, w4.at[i], w_sem.at[i])
        for i, src in enumerate((wq_hbm, wk_hbm, wv_hbm, wg_hbm))
    ]
    for copy in weights:
        copy.start()
    states = [
        pltpu.make_async_copy(
            state_hbm.at[pl.ds(i * GROUP, GROUP)],
            st.at[pl.ds(i * GROUP, GROUP)],
            st_sem.at[i],
        )
        for i in range(CHUNKS)
    ]
    for copy in states:
        copy.start()
    wo_copy = pltpu.make_async_copy(wo_hbm, wo, w_sem.at[4])
    wo_copy.start()
    for copy in small:
        copy.wait()

    x = tok[...].astype(F32)
    scale = lax.rsqrt(jnp.mean(x * x, axis=-1, keepdims=True) + EPS)
    normed = (x * scale * ngain[...]).astype(BF16)

    square = (ROWS, ROWS)
    place = jnp.sum(
        jnp.where(
            lax.broadcasted_iota(jnp.int32, square, 0) == lane_iota(square),
            jnp.broadcast_to(hist[...].astype(F32), square),
            0.0,
        ),
        axis=1,
        keepdims=True,
    )
    angles = place * inv[...]
    cosine = jnp.cos(angles)
    sine = jnp.sin(angles)

    zero = jnp.zeros((TILES, LANES), BF16)
    for e in range(EXPERTS):
        send0_ref[e] = zero
        send1_ref[e] = zero

    def project(i):
        weights[i].wait()
        return jnp.dot(normed, w4[i], preferred_element_type=F32).astype(BF16).astype(F32)

    q = rope(project(0), cosine, sine)
    qs[...] = q
    k = rope(project(1), cosine, sine) * (HD**-0.5)
    k_ref[...] = k
    v = project(2)
    v_ref[...] = v
    gate = project(3)

    ones = (
        lax.broadcasted_iota(jnp.int32, (RW, RW), 0) // HD == lane_iota((RW, RW)) // HD
    ).astype(BF16)
    fresh = group_sum(q * k, ones) * v
    heads = lane_iota((1, RW)) // HD
    rate = jnp.zeros((1, RW), F32)
    for h in range(HEADS):
        rate = jnp.where(heads == h, decay[h], rate)
    retain = jnp.exp(-rate)

    def chunk(i, carry):
        pltpu.make_async_copy(
            state_hbm.at[pl.ds(i * GROUP, GROUP)],
            st.at[pl.ds(i * GROUP, GROUP)],
            st_sem.at[i],
        ).wait()
        start = pl.multiple_of(i * GROUP, GROUP)
        qt = qs[pl.ds(start, GROUP), :].T
        for b in range(GROUP):
            for h in range(HEADS):
                column = qt[h * HD : (h + 1) * HD, b : b + 1]
                product = st[i * GROUP + b, h] * column
                total = product[0:8]
                for r in range(1, 8):
                    total = total + product[r * 8 : r * 8 + 8]
                part[
                    pl.ds(pl.multiple_of((h * ROWS + i * GROUP + b) * 8, 8), 8), 0:HD
                ] = total
        return carry

    lax.fori_loop(0, CHUNKS, chunk, 0)

    def head_rows(h):
        total = part[pl.ds(h * ROWS * 8, ROWS, stride=8), :]
        for s in range(1, 8):
            total = total + part[pl.ds(h * ROWS * 8 + s, ROWS, stride=8), :]
        return total

    low_half = lane_iota((ROWS, LANES)) < HD
    old = jnp.concatenate(
        [
            jnp.where(
                low_half, head_rows(2 * c), pltpu.roll(head_rows(2 * c + 1), HD, 1)
            )
            for c in range(HEADS // 2)
        ],
        axis=1,
    )
    reading = retain * old + fresh
    mean_square = group_sum(reading * reading, ones) * (1.0 / HD)
    reading = reading * lax.rsqrt(mean_square + EPS) * hgain[...]
    mixed_heads = (reading * jax.nn.silu(gate)).astype(BF16)
    wo_copy.wait()
    mixed = (x + jnp.dot(mixed_heads, wo[...], preferred_element_type=F32)).astype(BF16)
    mixed = mixed.astype(F32)
    scale = lax.rsqrt(jnp.mean(mixed * mixed, axis=-1, keepdims=True) + EPS)
    normed_moe = mixed * scale * mgain[...]

    for r in range(TILES):
        wide[pl.ds(r, ROWS, stride=TILES), :] = normed_moe[:, r * LANES : (r + 1) * LANES]
    tiles[...] = wide[...].astype(BF16).reshape(ROWS, TILES, LANES)
    for r in range(TILES):
        wide[pl.ds(r, ROWS, stride=TILES), :] = mixed[:, r * LANES : (r + 1) * LANES]
    mixed_ref[...] = wide[...].astype(BF16).reshape(ROWS, TILES, LANES)

    for t in range(ROWS):
        base = group[t] * PER_GROUP
        row = tiles[t]
        for j in range(2):
            send1_ref[base + inner[j, t]] = row
    for t in reversed(range(ROWS)):
        base = group[t] * PER_GROUP
        row = tiles[t]
        for j in (1, 0):
            send0_ref[base + inner[j, t]] = row


def state_kernel(
    decay, group, inner, weight, state_ref, k_ref, v_ref, new_ref, use_ref, seen
):
    kt = k_ref[...].T
    v = v_ref[...]
    for h in range(HEADS):
        retain = jnp.exp(jnp.full((HD, HD), -decay[h], F32))
        for b in range(GROUP):
            column = kt[h * HD : (h + 1) * HD, b : b + 1]
            row = v[b : b + 1, h * HD : (h + 1) * HD]
            new_ref[b, h] = retain * state_ref[b, h] + column * row

    @pl.when(pl.program_id(0) == 0)
    def _():
        def clear(e, carry):
            seen[e] = 0
            return carry

        lax.fori_loop(0, EXPERTS, clear, 0)

        def visit(t, carry):
            for j in range(2):
                e = group[t] * PER_GROUP + inner[j, t]
                slot = seen[e]
                seen[e] = 1
                w = weight[j, t]
                use_ref[0, j, t] = jnp.where(slot == 0, w, 0.0)
                use_ref[1, j, t] = jnp.where(slot == 0, 0.0, w)
            return carry

        lax.fori_loop(0, ROWS, visit, 0)


def expert_kernel(in_ref, wg_ref, wu_ref, wd_ref, out_ref, wide, lhs):
    n = in_ref.shape[0]
    wide[...] = in_ref[...].astype(F32).reshape(n * TILES, LANES)
    for r in range(TILES):
        lhs[:, r * LANES : (r + 1) * LANES] = wide[pl.ds(r, n, stride=TILES), :].astype(BF16)
    rows = lhs[...]
    gate = jnp.dot(rows, wg_ref[0], preferred_element_type=F32)
    up = jnp.dot(rows, wu_ref[0], preferred_element_type=F32)
    hidden = (jax.nn.silu(gate) * up).astype(BF16)
    out = jnp.dot(hidden, wd_ref[0], preferred_element_type=F32)
    for r in range(TILES):
        wide[pl.ds(r, n, stride=TILES), :] = out[:, r * LANES : (r + 1) * LANES]
    out_ref[...] = wide[...].astype(BF16).reshape(n, TILES, LANES)


def combine_kernel(group, inner, use, mixed_ref, back0_ref, back1_ref, out_ref, wide):
    for t in range(ROWS):
        total = mixed_ref[t].astype(F32)
        base = group[t] * PER_GROUP
        for j in range(2):
            e = base + inner[j, t]
            total = total + back0_ref[e].astype(F32) * use[0, j, t]
            total = total + back1_ref[e].astype(F32) * use[1, j, t]
        wide[t * TILES : (t + 1) * TILES, :] = total
    for r in range(TILES):
        out_ref[:, r * LANES : (r + 1) * LANES] = wide[
            pl.ds(r, ROWS, stride=TILES), :
        ].astype(BF16)


HBM = pl.BlockSpec(memory_space=pltpu.HBM)
VMEM = pl.BlockSpec(memory_space=pltpu.VMEM)
SMEM = pl.BlockSpec(memory_space=pltpu.SMEM)
ROW_TILES = (EXPERTS, TILES, LANES)


def local(
    tokens,
    history_length,
    norm_gain,
    w_query,
    w_key,
    w_value,
    w_gate,
    decay_rate,
    state,
    head_gain,
    w_out,
    moe_gain,
    route_weights,
    expert_group,
    expert_inner,
    expert_gate,
    expert_up,
    expert_down,
):
    inner = expert_inner.T
    inverse = jnp.asarray(
        (10000.0 ** (-(np.arange(LANES) % 32) / 32.0)).astype(np.float32).reshape(1, LANES)
    )
    mixed, send0, send1, keys, values = pl.pallas_call(
        front_kernel,
        out_shape=[
            jax.ShapeDtypeStruct((ROWS, TILES, LANES), BF16),
            jax.ShapeDtypeStruct(ROW_TILES, BF16),
            jax.ShapeDtypeStruct(ROW_TILES, BF16),
            jax.ShapeDtypeStruct((ROWS, RW), F32),
            jax.ShapeDtypeStruct((ROWS, RW), F32),
        ],
        in_specs=[HBM] * 15,
        out_specs=[VMEM] * 5,
        scratch_shapes=[
            pltpu.VMEM((1, ROWS), jnp.int32),
            pltpu.VMEM((1, LANES), F32),
            pltpu.VMEM((1, D), F32),
            pltpu.SMEM((HEADS,), F32),
            pltpu.VMEM((1, RW), F32),
            pltpu.VMEM((1, D), F32),
            pltpu.SMEM((ROWS,), jnp.int32),
            pltpu.SMEM((2, ROWS), jnp.int32),
            pltpu.VMEM((ROWS, D), BF16),
            pltpu.VMEM((4, D, RW), BF16),
            pltpu.VMEM((RW, D), BF16),
            pltpu.VMEM((ROWS, HEADS, HD, HD), F32),
            pltpu.VMEM((ROWS, RW), F32),
            pltpu.VMEM((HEADS * ROWS * 8, LANES), F32),
            pltpu.VMEM((ROWS * TILES, LANES), F32),
            pltpu.VMEM((ROWS, TILES, LANES), BF16),
            pltpu.SemaphoreType.DMA((9,)),
            pltpu.SemaphoreType.DMA((5,)),
            pltpu.SemaphoreType.DMA((CHUNKS,)),
        ],
        name="front",
    )(
        history_length.reshape(1, ROWS),
        inverse,
        norm_gain.reshape(1, D),
        decay_rate,
        head_gain.reshape(1, RW),
        moe_gain.reshape(1, D),
        expert_group,
        inner,
        tokens,
        w_query,
        w_key,
        w_value,
        w_gate,
        state,
        w_out,
    )
    new_state, use = pl.pallas_call(
        state_kernel,
        grid=(CHUNKS,),
        out_shape=[
            jax.ShapeDtypeStruct(state.shape, F32),
            jax.ShapeDtypeStruct((2, 2, ROWS), F32),
        ],
        in_specs=[
            SMEM,
            SMEM,
            SMEM,
            SMEM,
            pl.BlockSpec((GROUP, HEADS, HD, HD), lambda i: (i, 0, 0, 0)),
            pl.BlockSpec((GROUP, RW), lambda i: (i, 0)),
            pl.BlockSpec((GROUP, RW), lambda i: (i, 0)),
        ],
        out_specs=[
            pl.BlockSpec((GROUP, HEADS, HD, HD), lambda i: (i, 0, 0, 0)),
            SMEM,
        ],
        scratch_shapes=[pltpu.SMEM((EXPERTS,), jnp.int32)],
        cost_estimate=pl.CostEstimate(
            flops=10**9, bytes_accessed=26 * 10**6, transcendentals=0
        ),
        name="state_update",
    )(decay_rate, expert_group, inner, route_weights.T, state, keys, values)

    def dispatch(rows):
        return lax.all_to_all(rows, "ep", split_axis=0, concat_axis=0, tiled=True)

    expert = pl.pallas_call(
        expert_kernel,
        out_shape=jax.ShapeDtypeStruct(ROW_TILES, BF16),
        in_specs=[VMEM] * 4,
        out_specs=VMEM,
        scratch_shapes=[
            pltpu.VMEM((EXPERTS * TILES, LANES), F32),
            pltpu.VMEM((EXPERTS, D), BF16),
        ],
        cost_estimate=pl.CostEstimate(
            flops=4 * 10**8, bytes_accessed=4 * 10**6, transcendentals=0
        ),
        name="expert",
    )
    got0 = dispatch(send0)
    got1 = dispatch(send1)
    back0 = dispatch(expert(got0, expert_gate, expert_up, expert_down))
    back1 = dispatch(expert(got1, expert_gate, expert_up, expert_down))
    output = pl.pallas_call(
        combine_kernel,
        out_shape=jax.ShapeDtypeStruct((ROWS, D), BF16),
        in_specs=[SMEM, SMEM, SMEM, VMEM, VMEM, VMEM],
        out_specs=VMEM,
        scratch_shapes=[pltpu.VMEM((ROWS * TILES, LANES), F32)],
        name="combine",
    )(expert_group, inner, use, mixed, back0, back1)
    return output, new_state


def solution(mesh):
    return jax.shard_map(
        local,
        mesh=mesh,
        in_specs=(
            P("ep", None),
            P("ep"),
            P(),
            P(),
            P(),
            P(),
            P(),
            P(),
            P("ep", None, None, None),
            P(),
            P(),
            P(),
            P("ep", None),
            P("ep"),
            P("ep", None),
            P("ep", None, None),
            P("ep", None, None),
            P("ep", None, None),
        ),
        out_specs=(P("ep", None), P("ep", None, None, None)),
        check_vma=False,
    )
```

time: 105 us -> 106 us (level)
  Pallas kernels: 0 us -> 45.9 us
  matrix products: 20.3 us -> 0 us
  other arithmetic: 15.4 us -> 0 us
  local copies, waits for them, and re-layouts: 13 us -> 0.78 us
  starting transfers between devices: 4.52 us -> 13.8 us
  blocking collectives: 30.8 us -> 25.2 us
    pallas_call x0 -> x5, Pallas kernels: none -> 45.9 us  [the longest x1 21.8 us: local(): pl.pallas_call(state_kernel, grid=(CHUNKS,), out_shape=[jax.ShapeDtypeStr...]
    dot_general x9 -> x0, matrix products: 20.3 us -> none  [the longest x3 6.44 us: project(): jnp.dot(normed, weights, preferred_element_type=jnp.float32)]
    all_to_all x1 -> x3, starting transfers between devices: 4.52 us -> 13.8 us  [dispatch(): return lax.all_to_all(rows, 'ep', split_axis=0, concat_axis=0, tiled=True)]
    add x4 -> x0, other arithmetic: 9.18 us -> none  [the longest x1 8.48 us: retention_step(): retain[None, :, None, None] * state]
    reshape x6 -> x0, local copies, waits for them, and re-layouts: 7.74 us -> none  [the longest x1 2.56 us: local(): expert_apply(flat_rows, expert_gate[0], expert_up[0], expert_down[0])]
    all_to_all x1, blocking collectives: 30.8 us -> 25.2 us  [dispatch(): return lax.all_to_all(rows, 'ep', split_axis=0, concat_axis=0, tiled=True)]
    unnamed x16 -> x6, local copies, waits for them, and re-layouts: 3.43 us -> 0.78 us
    convert_element_type x4 -> x0, other arithmetic: 2.57 us -> none  [the longest x1 1.73 us: local(): output = (mixed_tokens.astype(jnp.float32) + routed).astype(jnp.bfloat16)]
  transfers between devices with their start and end apart: 1 -> 3, of which waited for: 1 -> 2; matrix products, arithmetic and copies ran while one was open for 0% -> 0% of each run, Pallas kernels for 0% -> 28%
where the time goes in v1:
time: 106 us
  Pallas kernels  45.9 us (43%)
  blocking collectives  25.2 us (24%)
  waiting for transfers between devices  19.2 us (18%)
  starting transfers between devices  13.8 us (13%)
    all_to_all x1, blocking collectives, dispatch(): return lax.all_to_all(rows, 'ep', split_axis=0, concat_axis=0, tiled=True)  25.2 us
    pallas_call x1, Pallas kernels, local(): pl.pallas_call(state_kernel, grid=(CHUNKS,), out_shape=[jax.ShapeDtypeStr...  21.8 us
    all_to_all x3, waiting for transfers between devices, dispatch(): return lax.all_to_all(rows, 'ep', split_axis=0, concat_axis=0, tiled=True)  19.2 us
    all_to_all x3, starting transfers between devices, dispatch(): return lax.all_to_all(rows, 'ep', split_axis=0, concat_axis=0, tiled=True)  13.8 us
    pallas_call x1, Pallas kernels, local(): pl.pallas_call(front_kernel, out_shape=[jax.ShapeDtypeStruct((ROWS, TILES...  13.8 us
    pallas_call x1, Pallas kernels, local(): back0 = dispatch(expert(got0, expert_gate, expert_up, expert_down))  4 us
    pallas_call x1, Pallas kernels, local(): back1 = dispatch(expert(got1, expert_gate, expert_up, expert_down))  3.99 us
    pallas_call x1, Pallas kernels, local(): pl.pallas_call(combine_kernel, out_shape=jax.ShapeDtypeStruct((ROWS, D),...  2.27 us
  transfers between devices with their start and end apart: 3, of which 2 were waited for; matrix products, arithmetic and copies ran while one was open for 0% of the time, Pallas kernels for 28%

profile of v1, /device:TPU:1, one launch (start us, length us, event | category | flops | bytes accessed | tf_op | source)
XLA Modules:
  0.0 105.6 jit_solution(1371183257374195537)
XLA Ops:
  0.6 13.8 %front.1 = (bf16[48,16,128]{2,1,0:T(8,128)(2,1)}, bf16[128,16,128]{2,1,0:T(8,128)(2,1)}, bf16[128,16,128]{2,1,0:T(8,128)(2,1)}, f32[48,512]{1,0:T(8,128)}, f32[48,512]{1,0:T(8,128)}) custom-call(s32[1,48]{1,0:T(1,128)} %bitcast.13, f32[1,128]{1,0:T(1,128)} %constant.2.clone.inv_hbm, f32[1,2048]{1,0:T(1,128)} %bitcast.9, f32[8]{0:T(128)} %decay.1, ...), custom_call_target="tpu_custom_call" | custom-call | tf_op jit(solution)/shard_map/front/pallas_call | solution.py:334
  14.4 25.2 %all_to_all.20.in_ref = bf16[128,16,128]{2,1,0:T(8,128)(2,1)} all-to-all(bf16[128,16,128]{2,1,0:T(8,128)(2,1)} %get-tuple-element.13), channel_id=1, replica_groups=mesh['ep'=128] {'ep'}, dimensions={0} | all-to-all | bytes 1048576 | tf_op jit(solution)/shard_map/all_to_all | solution.py:412
  39.7 4.6 %all-to-all-start.2 = ((bf16[128,16,128]{2,1,0:T(8,128)(2,1)}), bf16[128,16,128]{2,1,0:T(8,128)(2,1)S(1)}, u32[]{:S(2)}, u32[]{:S(2)}) async-start(bf16[128,16,128]{2,1,0:T(8,128)(2,1)} %get-tuple-element.14), calls=%async_computation.2 | async-start | bytes 1048576 | tf_op jit(solution)/shard_map/all_to_all | solution.py:412
  44.3 4.0 %expert.2 = bf16[128,16,128]{2,1,0:T(8,128)(2,1)} custom-call(bf16[128,16,128]{2,1,0:T(8,128)(2,1)} %all_to_all.20.in_ref, bf16[1,2048,256]{2,1,0:T(8,128)(2,1)} %wg_ref.3, bf16[1,2048,256]{2,1,0:T(8,128)(2,1)} %wu_ref.3, bf16[1,256,2048]{2,1,0:T(8,128)(2,1)} %wd_ref.3), custom_call_target="tpu_custom_call" | custom-call | flops 400000000 | bytes 4000000 | tf_op jit(solution)/shard_map/expert/pallas_call | solution.py:430
  48.3 9.6 %all-to-all-done.2.in_ref = bf16[128,16,128]{2,1,0:T(8,128)(2,1)S(1)} async-done(((bf16[128,16,128]{2,1,0:T(8,128)(2,1)}), bf16[128,16,128]{2,1,0:T(8,128)(2,1)S(1)}, u32[]{:S(2)}, u32[]{:S(2)}) %all-to-all-start.2) | async-done | bytes 524320 | tf_op jit(solution)/shard_map/all_to_all | solution.py:412
  57.9 0.0 copy-start.2
  57.9 4.6 %all-to-all-start.1 = ((bf16[128,16,128]{2,1,0:T(8,128)(2,1)}), bf16[128,16,128]{2,1,0:T(8,128)(2,1)S(1)}, u32[]{:S(2)}, u32[]{:S(2)}) async-start(bf16[128,16,128]{2,1,0:T(8,128)(2,1)} %expert.2), calls=%async_computation.1 | async-start | bytes 1048576 | tf_op jit(solution)/shard_map/all_to_all | solution.py:412
  62.5 0.0 copy-done.2
  62.5 4.0 %expert.3 = bf16[128,16,128]{2,1,0:T(8,128)(2,1)} custom-call(bf16[128,16,128]{2,1,0:T(8,128)(2,1)} %copy-done.2, bf16[1,2048,256]{2,1,0:T(8,128)(2,1)} %wg_ref.3, bf16[1,2048,256]{2,1,0:T(8,128)(2,1)} %wu_ref.3, bf16[1,256,2048]{2,1,0:T(8,128)(2,1)} %wd_ref.3), custom_call_target="tpu_custom_call" | custom-call | flops 400000000 | bytes 4000000 | tf_op jit(solution)/shard_map/expert/pallas_call | solution.py:431
  66.5 9.6 %all-to-all-done.1.back0_ref = bf16[128,16,128]{2,1,0:T(8,128)(2,1)S(1)} async-done(((bf16[128,16,128]{2,1,0:T(8,128)(2,1)}), bf16[128,16,128]{2,1,0:T(8,128)(2,1)S(1)}, u32[]{:S(2)}, u32[]{:S(2)}) %all-to-all-start.1) | async-done | bytes 524320 | tf_op jit(solution)/shard_map/all_to_all | solution.py:412
  76.1 0.0 copy-start
  76.1 4.6 %all-to-all-start.3 = ((bf16[128,16,128]{2,1,0:T(8,128)(2,1)}), bf16[128,16,128]{2,1,0:T(8,128)(2,1)S(1)}, u32[]{:S(2)}, u32[]{:S(2)}) async-start(bf16[128,16,128]{2,1,0:T(8,128)(2,1)} %expert.3), calls=%async_computation.3 | async-start | bytes 1048576 | tf_op jit(solution)/shard_map/all_to_all | solution.py:412
  80.7 21.8 %state_update.1 = (f32[48,8,64,64]{3,2,1,0:T(8,128)}, f32[2,2,48]{2,1,0:T(2,128)}) custom-call(f32[8]{0:T(128)} %decay.1, s32[48]{0:T(128)} %group.3, s32[2,48]{1,0:T(2,128)} %bitcast.7, f32[2,48]{1,0:T(2,128)} %bitcast.12, f32[48,8,64,64]{3,2,1,0:T(8,128)} %state_ref.1, f32[48,512]{1,0:T(8,128)} %get-tuple-element.9.k_ref, f32[48,512]{1,0:T(8,128)} %get-tuple-element.10.v_ref), custom_call_target="tpu_custom_call" | custom-call | flops 1000000000 | bytes 26000000 | tf_op jit(solution)/shard_map/state_update/pallas_call | solution.py:384
  102.5 0.0 copy-done
  102.5 0.0 all-to-all-done.3.back1_ref
  102.5 0.0 copy-start.1
  102.5 0.8 copy-done.1
  103.3 2.3 %combine.1 = bf16[48,2048]{1,0:T(8,128)(2,1)} custom-call(s32[48]{0:T(128)} %group.3, s32[2,48]{1,0:T(2,128)} %bitcast.8, f32[2,2,48]{2,1,0:T(2,128)} %get-tuple-element.11.use, bf16[48,16,128]{2,1,0:T(8,128)(2,1)} %get-tuple-element.12.mixed_ref, bf16[128,16,128]{2,1,0:T(8,128)(2,1)} %copy-done, bf16[128,16,128]{2,1,0:T(8,128)(2,1)} %copy-done.1), custom_call_target="tpu_custom_call" | custom-call | tf_op jit(solution)/shard_map/combine/pallas_call | solution.py:432
Async XLA Ops:
  39.7 18.2 %all-to-all-start.2 = ((bf16[128,16,128]{2,1,0:T(8,128)(2,1)}), bf16[128,16,128]{2,1,0:T(8,128)(2,1)S(1)}, u32[]{:S(2)}, u32[]{:S(2)}) async-start(bf16[128,16,128]{2,1,0:T(8,128)(2,1)} %get-tuple-element.14), calls=%async_computation.2 | async-start | bytes 1048576 | tf_op jit(solution)/shard_map/all_to_all | solution.py:412
  57.9 4.6 %copy-start.2 = (bf16[128,16,128]{2,1,0:T(8,128)(2,1)}, bf16[128,16,128]{2,1,0:T(8,128)(2,1)S(1)}, u32[]{:S(2)}) copy-start(bf16[128,16,128]{2,1,0:T(8,128)(2,1)S(1)} %all-to-all-done.2.in_ref) | copy-start | bytes 1572868
  57.9 18.2 %all-to-all-start.1 = ((bf16[128,16,128]{2,1,0:T(8,128)(2,1)}), bf16[128,16,128]{2,1,0:T(8,128)(2,1)S(1)}, u32[]{:S(2)}, u32[]{:S(2)}) async-start(bf16[128,16,128]{2,1,0:T(8,128)(2,1)} %expert.2), calls=%async_computation.1 | async-start | bytes 1048576 | tf_op jit(solution)/shard_map/all_to_all | solution.py:412
  76.1 26.4 %copy-start = (bf16[128,16,128]{2,1,0:T(8,128)(2,1)}, bf16[128,16,128]{2,1,0:T(8,128)(2,1)S(1)}, u32[]{:S(2)}) copy-start(bf16[128,16,128]{2,1,0:T(8,128)(2,1)S(1)} %all-to-all-done.1.back0_ref) | copy-start | bytes 1572868
  76.1 26.4 %all-to-all-start.3 = ((bf16[128,16,128]{2,1,0:T(8,128)(2,1)}), bf16[128,16,128]{2,1,0:T(8,128)(2,1)S(1)}, u32[]{:S(2)}, u32[]{:S(2)}) async-start(bf16[128,16,128]{2,1,0:T(8,128)(2,1)} %expert.3), calls=%async_computation.3 | async-start | bytes 1048576 | tf_op jit(solution)/shard_map/all_to_all | solution.py:412
  102.5 0.8 copy-start.1

commit v2 on v1

--- a/solution.py
+++ b/solution.py
@@ -68,8 +68,7 @@
     state_hbm,
     wo_hbm,
     mixed_ref,
-    send0_ref,
-    send1_ref,
+    send_ref,
     k_ref,
     v_ref,
     hist,
@@ -111,6 +110,8 @@
     ]
     for copy in weights:
         copy.start()
+    wo_copy = pltpu.make_async_copy(wo_hbm, wo, w_sem.at[4])
+    wo_copy.start()
     states = [
         pltpu.make_async_copy(
             state_hbm.at[pl.ds(i * GROUP, GROUP)],
@@ -121,8 +122,6 @@
     ]
     for copy in states:
         copy.start()
-    wo_copy = pltpu.make_async_copy(wo_hbm, wo, w_sem.at[4])
-    wo_copy.start()
     for copy in small:
         copy.wait()
 
@@ -145,16 +144,17 @@
     sine = jnp.sin(angles)
 
     zero = jnp.zeros((TILES, LANES), BF16)
-    for e in range(EXPERTS):
-        send0_ref[e] = zero
-        send1_ref[e] = zero
+    for e in range(2 * EXPERTS):
+        send_ref[e] = zero
 
     def project(i):
         weights[i].wait()
         return jnp.dot(normed, w4[i], preferred_element_type=F32).astype(BF16).astype(F32)
 
     q = rope(project(0), cosine, sine)
-    qs[...] = q
+    high = q.astype(BF16).astype(F32)
+    qs[0] = high
+    qs[1] = q - high
     k = rope(project(1), cosine, sine) * (HD**-0.5)
     k_ref[...] = k
     v = project(2)
@@ -171,33 +171,36 @@
         rate = jnp.where(heads == h, decay[h], rate)
     retain = jnp.exp(-rate)
 
+    own = (
+        lax.broadcasted_iota(jnp.int32, (HEADS, RW), 0) == lane_iota((HEADS, RW)) // HD
+    )
+
     def chunk(i, carry):
         pltpu.make_async_copy(
             state_hbm.at[pl.ds(i * GROUP, GROUP)],
             st.at[pl.ds(i * GROUP, GROUP)],
             st_sem.at[i],
         ).wait()
-        start = pl.multiple_of(i * GROUP, GROUP)
-        qt = qs[pl.ds(start, GROUP), :].T
         for b in range(GROUP):
-            for h in range(HEADS):
-                column = qt[h * HD : (h + 1) * HD, b : b + 1]
-                product = st[i * GROUP + b, h] * column
-                total = product[0:8]
-                for r in range(1, 8):
-                    total = total + product[r * 8 : r * 8 + 8]
-                part[
-                    pl.ds(pl.multiple_of((h * ROWS + i * GROUP + b) * 8, 8), 8), 0:HD
-                ] = total
+            t = i * GROUP + b
+            spread = [
+                jnp.where(own, jnp.broadcast_to(qs[s, pl.ds(t, 1), :], (HEADS, RW)), 0.0)
+                for s in range(2)
+            ]
+            total = jnp.dot(
+                jnp.concatenate(spread, axis=0).astype(BF16),
+                st[t].reshape(RW, HD).astype(BF16),
+                preferred_element_type=F32,
+            )
+            part[pl.ds(pl.multiple_of(t * HEADS, HEADS), HEADS), 0:HD] = (
+                total[0:HEADS] + total[HEADS:]
+            )
         return carry
 
     lax.fori_loop(0, CHUNKS, chunk, 0)
 
     def head_rows(h):
-        total = part[pl.ds(h * ROWS * 8, ROWS, stride=8), :]
-        for s in range(1, 8):
-            total = total + part[pl.ds(h * ROWS * 8 + s, ROWS, stride=8), :]
-        return total
+        return part[pl.ds(h, ROWS, stride=HEADS), :]
 
     low_half = lane_iota((ROWS, LANES)) < HD
     old = jnp.concatenate(
@@ -230,25 +233,41 @@
         base = group[t] * PER_GROUP
         row = tiles[t]
         for j in range(2):
-            send1_ref[base + inner[j, t]] = row
+            send_ref[(base + inner[j, t]) * 2 + 1] = row
     for t in reversed(range(ROWS)):
         base = group[t] * PER_GROUP
         row = tiles[t]
         for j in (1, 0):
-            send0_ref[base + inner[j, t]] = row
-
-
-def state_kernel(
-    decay, group, inner, weight, state_ref, k_ref, v_ref, new_ref, use_ref, seen
-):
-    kt = k_ref[...].T
+            send_ref[(base + inner[j, t]) * 2] = row
+
+
+def state_kernel(decay, group, inner, state_ref, k_ref, v_ref, new_ref, slot_ref, seen):
+    k = k_ref[...]
+    high = k.astype(BF16).astype(F32)
+    kt = jnp.concatenate([high, k - high], axis=0).T.astype(BF16)
     v = v_ref[...]
-    for h in range(HEADS):
-        retain = jnp.exp(jnp.full((HD, HD), -decay[h], F32))
-        for b in range(GROUP):
-            column = kt[h * HD : (h + 1) * HD, b : b + 1]
-            row = v[b : b + 1, h * HD : (h + 1) * HD]
-            new_ref[b, h] = retain * state_ref[b, h] + column * row
+    swapped = jnp.concatenate(
+        [
+            pltpu.roll(v[:, c * LANES : (c + 1) * LANES], HD, 1)
+            for c in range(RW // LANES)
+        ],
+        axis=1,
+    )
+    retains = [jnp.exp(jnp.full((HD, HD), -decay[h], F32)) for h in range(HEADS)]
+    for pair in range(GROUP // 2):
+        shape = (2 * GROUP, 2 * LANES)
+        pick = (
+            lax.broadcasted_iota(jnp.int32, shape, 0) % GROUP
+            == lane_iota(shape) // LANES + 2 * pair
+        ).astype(BF16)
+        columns = jnp.dot(kt, pick, preferred_element_type=F32)
+        for i in range(2):
+            b = 2 * pair + i
+            for h in range(HEADS):
+                column = columns[h * HD : (h + 1) * HD, i * LANES : i * LANES + HD]
+                c = (h // 2) * LANES
+                row = (swapped if h % 2 else v)[b : b + 1, c : c + HD]
+                new_ref[b, h] = retains[h] * state_ref[b, h] + column * row
 
     @pl.when(pl.program_id(0) == 0)
     def _():
@@ -261,11 +280,8 @@
         def visit(t, carry):
             for j in range(2):
                 e = group[t] * PER_GROUP + inner[j, t]
-                slot = seen[e]
+                slot_ref[j, t] = 2 * e + seen[e]
                 seen[e] = 1
-                w = weight[j, t]
-                use_ref[0, j, t] = jnp.where(slot == 0, w, 0.0)
-                use_ref[1, j, t] = jnp.where(slot == 0, 0.0, w)
             return carry
 
         lax.fori_loop(0, ROWS, visit, 0)
@@ -286,14 +302,11 @@
     out_ref[...] = wide[...].astype(BF16).reshape(n, TILES, LANES)
 
 
-def combine_kernel(group, inner, use, mixed_ref, back0_ref, back1_ref, out_ref, wide):
+def combine_kernel(slot, weight, mixed_ref, back_ref, out_ref, wide):
     for t in range(ROWS):
         total = mixed_ref[t].astype(F32)
-        base = group[t] * PER_GROUP
         for j in range(2):
-            e = base + inner[j, t]
-            total = total + back0_ref[e].astype(F32) * use[0, j, t]
-            total = total + back1_ref[e].astype(F32) * use[1, j, t]
+            total = total + back_ref[slot[j, t]].astype(F32) * weight[j, t]
         wide[t * TILES : (t + 1) * TILES, :] = total
     for r in range(TILES):
         out_ref[:, r * LANES : (r + 1) * LANES] = wide[
@@ -301,10 +314,18 @@
         ].astype(BF16)
 
 
+def in_vmem(x):
+    return pltpu.with_memory_space_constraint(x, pltpu.VMEM)
+
+
+def in_hbm(x):
+    return pltpu.with_memory_space_constraint(x, pltpu.HBM)
+
+
 HBM = pl.BlockSpec(memory_space=pltpu.HBM)
 VMEM = pl.BlockSpec(memory_space=pltpu.VMEM)
 SMEM = pl.BlockSpec(memory_space=pltpu.SMEM)
-ROW_TILES = (EXPERTS, TILES, LANES)
+ROW_TILES = (2 * EXPERTS, TILES, LANES)
 
 
 def local(
@@ -331,17 +352,16 @@
     inverse = jnp.asarray(
         (10000.0 ** (-(np.arange(LANES) % 32) / 32.0)).astype(np.float32).reshape(1, LANES)
     )
-    mixed, send0, send1, keys, values = pl.pallas_call(
+    mixed, send, keys, values = pl.pallas_call(
         front_kernel,
         out_shape=[
-            jax.ShapeDtypeStruct((ROWS, TILES, LANES), BF16),
-            jax.ShapeDtypeStruct(ROW_TILES, BF16),
-            jax.ShapeDtypeStruct(ROW_TILES, BF16),
-            jax.ShapeDtypeStruct((ROWS, RW), F32),
-            jax.ShapeDtypeStruct((ROWS, RW), F32),
+            pltpu.VMEM((ROWS, TILES, LANES), BF16),
+            pltpu.VMEM(ROW_TILES, BF16),
+            pltpu.VMEM((ROWS, RW), F32),
+            pltpu.VMEM((ROWS, RW), F32),
         ],
         in_specs=[HBM] * 15,
-        out_specs=[VMEM] * 5,
+        out_specs=[VMEM] * 4,
         scratch_shapes=[
             pltpu.VMEM((1, ROWS), jnp.int32),
             pltpu.VMEM((1, LANES), F32),
@@ -355,41 +375,46 @@
             pltpu.VMEM((4, D, RW), BF16),
             pltpu.VMEM((RW, D), BF16),
             pltpu.VMEM((ROWS, HEADS, HD, HD), F32),
-            pltpu.VMEM((ROWS, RW), F32),
-            pltpu.VMEM((HEADS * ROWS * 8, LANES), F32),
+            pltpu.VMEM((2, ROWS, RW), F32),
+            pltpu.VMEM((HEADS * ROWS, LANES), F32),
             pltpu.VMEM((ROWS * TILES, LANES), F32),
             pltpu.VMEM((ROWS, TILES, LANES), BF16),
             pltpu.SemaphoreType.DMA((9,)),
             pltpu.SemaphoreType.DMA((5,)),
             pltpu.SemaphoreType.DMA((CHUNKS,)),
         ],
+        compiler_params=pltpu.CompilerParams(vmem_limit_bytes=36 * 2**20),
         name="front",
     )(
-        history_length.reshape(1, ROWS),
-        inverse,
-        norm_gain.reshape(1, D),
-        decay_rate,
-        head_gain.reshape(1, RW),
-        moe_gain.reshape(1, D),
-        expert_group,
-        inner,
-        tokens,
-        w_query,
-        w_key,
-        w_value,
-        w_gate,
-        state,
-        w_out,
-    )
-    new_state, use = pl.pallas_call(
+        *(
+            in_hbm(x)
+            for x in (
+                history_length.reshape(1, ROWS),
+                inverse,
+                norm_gain.reshape(1, D),
+                decay_rate,
+                head_gain.reshape(1, RW),
+                moe_gain.reshape(1, D),
+                expert_group,
+                inner,
+                tokens,
+                w_query,
+                w_key,
+                w_value,
+                w_gate,
+                state,
+                w_out,
+            )
+        )
+    )
+    new_state, slots = pl.pallas_call(
         state_kernel,
         grid=(CHUNKS,),
         out_shape=[
             jax.ShapeDtypeStruct(state.shape, F32),
-            jax.ShapeDtypeStruct((2, 2, ROWS), F32),
+            jax.ShapeDtypeStruct((2, ROWS), jnp.int32),
         ],
         in_specs=[
-            SMEM,
             SMEM,
             SMEM,
             SMEM,
@@ -405,38 +430,49 @@
         cost_estimate=pl.CostEstimate(
             flops=10**9, bytes_accessed=26 * 10**6, transcendentals=0
         ),
+        compiler_params=pltpu.CompilerParams(vmem_limit_bytes=20 * 2**20),
         name="state_update",
-    )(decay_rate, expert_group, inner, route_weights.T, state, keys, values)
+    )(
+        in_hbm(decay_rate),
+        in_hbm(expert_group),
+        in_hbm(inner),
+        in_hbm(state),
+        in_vmem(keys),
+        in_vmem(values),
+    )
 
     def dispatch(rows):
         return lax.all_to_all(rows, "ep", split_axis=0, concat_axis=0, tiled=True)
 
-    expert = pl.pallas_call(
+    outputs = pl.pallas_call(
         expert_kernel,
-        out_shape=jax.ShapeDtypeStruct(ROW_TILES, BF16),
+        out_shape=pltpu.VMEM(ROW_TILES, BF16),
         in_specs=[VMEM] * 4,
         out_specs=VMEM,
         scratch_shapes=[
-            pltpu.VMEM((EXPERTS * TILES, LANES), F32),
-            pltpu.VMEM((EXPERTS, D), BF16),
+            pltpu.VMEM((2 * EXPERTS * TILES, LANES), F32),
+            pltpu.VMEM((2 * EXPERTS, D), BF16),
         ],
         cost_estimate=pl.CostEstimate(
-            flops=4 * 10**8, bytes_accessed=4 * 10**6, transcendentals=0
+            flops=8 * 10**8, bytes_accessed=4 * 10**6, transcendentals=0
         ),
+        compiler_params=pltpu.CompilerParams(vmem_limit_bytes=16 * 2**20),
         name="expert",
-    )
-    got0 = dispatch(send0)
-    got1 = dispatch(send1)
-    back0 = dispatch(expert(got0, expert_gate, expert_up, expert_down))
-    back1 = dispatch(expert(got1, expert_gate, expert_up, expert_down))
+    )(
+        in_vmem(dispatch(send)),
+        in_vmem(expert_gate),
+        in_vmem(expert_up),
+        in_vmem(expert_down),
+    )
     output = pl.pallas_call(
         combine_kernel,
         out_shape=jax.ShapeDtypeStruct((ROWS, D), BF16),
-        in_specs=[SMEM, SMEM, SMEM, VMEM, VMEM, VMEM],
+        in_specs=[SMEM, SMEM, VMEM, VMEM],
         out_specs=VMEM,
         scratch_shapes=[pltpu.VMEM((ROWS * TILES, LANES), F32)],
+        compiler_params=pltpu.CompilerParams(vmem_limit_bytes=8 * 2**20),
         name="combine",
-    )(expert_group, inner, use, mixed, back0, back1)
+    )(slots, in_hbm(route_weights.T), in_vmem(mixed), in_vmem(dispatch(outputs)))
     return output, new_state
 
 

time: 106 us -> 69.6 us (0.66)
  Pallas kernels: 45.9 us -> 27.1 us
  waiting for transfers between devices: 19.2 us -> 6.61 us
  starting transfers between devices: 13.8 us -> 4.43 us
  blocking collectives: 25.2 us -> 30.5 us
    all_to_all x3 -> x1, waiting for transfers between devices: 19.2 us -> 6.61 us  [dispatch(): return lax.all_to_all(rows, 'ep', split_axis=0, concat_axis=0, tiled=True)]
    all_to_all x3 -> x1, starting transfers between devices: 13.8 us -> 4.43 us  [dispatch(): return lax.all_to_all(rows, 'ep', split_axis=0, concat_axis=0, tiled=True)]
    pallas_call x1, Pallas kernels: 21.8 us -> 12.7 us  [local(): pl.pallas_call(state_kernel, grid=(CHUNKS,), out_shape=[jax.ShapeDtypeStr...]
    pallas_call x3 -> x2, Pallas kernels: 21.8 us -> 12.8 us  [the longest x1 9.74 us: local(): pl.pallas_call(front_kernel, out_shape=[pltpu.VMEM((ROWS, TILES, LANES),...]
    all_to_all x1, blocking collectives: 25.2 us -> 30.5 us  [dispatch(): return lax.all_to_all(rows, 'ep', split_axis=0, concat_axis=0, tiled=True)]
  transfers between devices with their start and end apart: 3 -> 1, of which waited for: 2 -> 1; matrix products, arithmetic and copies ran while one was open for 0% -> 0% of each run, Pallas kernels for 28% -> 18%
where the time goes in v2:
time: 69.6 us; the launch traced here: 69.4 us
  blocking collectives  30.5 us (44%)
  Pallas kernels  27.1 us (39%)
  waiting for transfers between devices  6.61 us (9%)
  starting transfers between devices  4.43 us (6%)
    all_to_all x1, blocking collectives, dispatch(): return lax.all_to_all(rows, 'ep', split_axis=0, concat_axis=0, tiled=True)  30.5 us
    pallas_call x1, Pallas kernels, local(): pl.pallas_call(state_kernel, grid=(CHUNKS,), out_shape=[jax.ShapeDtypeStr...  12.7 us
    pallas_call x1, Pallas kernels, local(): pl.pallas_call(front_kernel, out_shape=[pltpu.VMEM((ROWS, TILES, LANES),...  9.74 us
    all_to_all x1, waiting for transfers between devices, dispatch(): return lax.all_to_all(rows, 'ep', split_axis=0, concat_axis=0, tiled=True)  6.61 us
    all_to_all x1, starting transfers between devices, dispatch(): return lax.all_to_all(rows, 'ep', split_axis=0, concat_axis=0, tiled=True)  4.43 us
    pallas_call x1, Pallas kernels, local(): pl.pallas_call(expert_kernel, out_shape=pltpu.VMEM(ROW_TILES, BF16), in_s...  3.05 us
    pallas_call x1, Pallas kernels, local(): pl.pallas_call(combine_kernel, out_shape=jax.ShapeDtypeStruct((ROWS, D),...  1.62 us
  transfers between devices with their start and end apart: 1, of which 1 were waited for; matrix products, arithmetic and copies ran while one was open for 0% of the time, Pallas kernels for 18%

profile of v2, /device:TPU:1, one launch (start us, length us, event | category | flops | bytes accessed | tf_op | source)
XLA Modules:
  0.0 69.4 jit_solution(1672818748399120263)
XLA Ops:
  0.6 0.0 copy-start.2
  0.6 9.7 %front.1 = (bf16[48,16,128]{2,1,0:T(8,128)(2,1)S(1)}, bf16[256,16,128]{2,1,0:T(8,128)(2,1)S(1)}, f32[48,512]{1,0:T(8,128)S(1)}, f32[48,512]{1,0:T(8,128)S(1)}) custom-call(s32[1,48]{1,0:T(1,128)} %bitcast.12, f32[1,128]{1,0:T(1,128)} %constant.2.clone.inv_hbm, f32[1,2048]{1,0:T(1,128)} %bitcast.6, f32[8]{0:T(128)} %decay.1, f32[1,512]{1,0:T(1,128)} %bitcast.10, ...), custom_call_target="tpu_custom_call" | custom-call | tf_op jit(solution)/shard_map/front/pallas_call | solution.py:355
  10.4 0.0 copy-start
  10.4 0.0 copy-start.1
  10.4 30.5 %all_to_all.10.in_ref = bf16[256,16,128]{2,1,0:T(8,128)(2,1)S(1)} all-to-all(bf16[256,16,128]{2,1,0:T(8,128)(2,1)S(1)} %get-tuple-element.12), channel_id=1, replica_groups=mesh['ep'=128] {'ep'}, dimensions={0} | all-to-all | bytes 2097152 | tf_op jit(solution)/shard_map/all_to_all | solution.py:445
  40.9 0.0 copy-done.2
  40.9 0.0 copy-done
  40.9 0.0 copy-done.1
  40.9 3.1 %expert.1 = bf16[256,16,128]{2,1,0:T(8,128)(2,1)} custom-call(bf16[256,16,128]{2,1,0:T(8,128)(2,1)S(1)} %all_to_all.10.in_ref, bf16[1,2048,256]{2,1,0:T(8,128)(2,1)S(1)} %copy-done, bf16[1,2048,256]{2,1,0:T(8,128)(2,1)S(1)} %copy-done.1, bf16[1,256,2048]{2,1,0:T(8,128)(2,1)S(1)} %copy-done.2), custom_call_target="tpu_custom_call" | custom-call | flops 800000000 | bytes 4000000 | tf_op jit(solution)/shard_map/expert/pallas_call | solution.py:447
  44.0 4.4 %all-to-all-start.1 = ((bf16[256,16,128]{2,1,0:T(8,128)(2,1)}), bf16[256,16,128]{2,1,0:T(8,128)(2,1)S(1)}, u32[]{:S(2)}, u32[]{:S(2)}) async-start(bf16[256,16,128]{2,1,0:T(8,128)(2,1)} %expert.1), calls=%async_computation.1 | async-start | bytes 2097152 | tf_op jit(solution)/shard_map/all_to_all | solution.py:445
  48.4 12.7 %state_update.1 = (f32[48,8,64,64]{3,2,1,0:T(8,128)}, s32[2,48]{1,0:T(2,128)S(1)}) custom-call(f32[8]{0:T(128)} %decay.1, s32[48]{0:T(128)} %group.1, s32[2,48]{1,0:T(2,128)} %bitcast.9, f32[48,8,64,64]{3,2,1,0:T(8,128)} %state_ref.1, f32[48,512]{1,0:T(8,128)S(1)} %get-tuple-element.8.k_ref, f32[48,512]{1,0:T(8,128)S(1)} %get-tuple-element.9.v_ref), custom_call_target="tpu_custom_call" | custom-call | flops 1000000000 | bytes 26000000 | tf_op jit(solution)/shard_map/state_update/pallas_call | solution.py:410
  61.1 6.6 %all-to-all-done.1.back_ref = bf16[256,16,128]{2,1,0:T(8,128)(2,1)S(1)} async-done(((bf16[256,16,128]{2,1,0:T(8,128)(2,1)}), bf16[256,16,128]{2,1,0:T(8,128)(2,1)S(1)}, u32[]{:S(2)}, u32[]{:S(2)}) %all-to-all-start.1) | async-done | bytes 1048608 | tf_op jit(solution)/shard_map/all_to_all | solution.py:445
  67.7 1.6 %combine.1 = bf16[48,2048]{1,0:T(8,128)(2,1)} custom-call(s32[2,48]{1,0:T(2,128)S(1)} %get-tuple-element.10.slot, f32[2,48]{1,0:T(2,128)} %bitcast.11, bf16[48,16,128]{2,1,0:T(8,128)(2,1)S(1)} %get-tuple-element.11.mixed_ref, bf16[256,16,128]{2,1,0:T(8,128)(2,1)S(1)} %all-to-all-done.1.back_ref), custom_call_target="tpu_custom_call" | custom-call | tf_op jit(solution)/shard_map/combine/pallas_call | solution.py:467
Async XLA Ops:
  0.6 40.3 %copy-start.2 = (bf16[1,256,2048]{2,1,0:T(8,128)(2,1)S(1)}, bf16[1,256,2048]{2,1,0:T(8,128)(2,1)}, u32[]{:S(2)}) copy-start(bf16[1,256,2048]{2,1,0:T(8,128)(2,1)} %wd_ref.1) | copy-start | bytes 3145732
  10.4 30.5 %copy-start = (bf16[1,2048,256]{2,1,0:T(8,128)(2,1)S(1)}, bf16[1,2048,256]{2,1,0:T(8,128)(2,1)}, u32[]{:S(2)}) copy-start(bf16[1,2048,256]{2,1,0:T(8,128)(2,1)} %wg_ref.1) | copy-start | bytes 3145732
  10.4 30.5 %copy-start.1 = (bf16[1,2048,256]{2,1,0:T(8,128)(2,1)S(1)}, bf16[1,2048,256]{2,1,0:T(8,128)(2,1)}, u32[]{:S(2)}) copy-start(bf16[1,2048,256]{2,1,0:T(8,128)(2,1)} %wu_ref.1) | copy-start | bytes 3145732
  44.0 23.7 %all-to-all-start.1 = ((bf16[256,16,128]{2,1,0:T(8,128)(2,1)}), bf16[256,16,128]{2,1,0:T(8,128)(2,1)S(1)}, u32[]{:S(2)}, u32[]{:S(2)}) async-start(bf16[256,16,128]{2,1,0:T(8,128)(2,1)} %expert.1), calls=%async_computation.1 | async-start | bytes 2097152 | tf_op jit(solution)/shard_map/all_to_all | solution.py:445

commit v3 on v2

v3 whole, which is shorter than its diff:
```python
import functools

import jax
import jax.numpy as jnp
import numpy as np
from jax import lax
from jax.experimental import pallas as pl
from jax.experimental.pallas import tpu as pltpu
from jax.sharding import PartitionSpec as P

EPS = 1e-06
ROWS = 48
D = 2048
HEADS = 8
HD = 64
RW = HEADS * HD
EXPERTS = 128
PER_GROUP = 32
LANES = 128
TILES = D // LANES
GROUP = 8
CHUNKS = ROWS // GROUP
BLOCK = 128
PART = 16
F32 = jnp.float32
BF16 = jnp.bfloat16


def lane_iota(shape):
    return lax.broadcasted_iota(jnp.int32, shape, len(shape) - 1)


def row_iota(shape):
    return lax.broadcasted_iota(jnp.int32, shape, 0)


def split(x):
    high = x.astype(BF16).astype(F32)
    return high, x - high


def by_lanes(f, x):
    return jnp.concatenate(
        [f(x[:, c * LANES : (c + 1) * LANES]) for c in range(x.shape[1] // LANES)],
        axis=1,
    )


def head_sum(x):
    shape = (LANES, LANES)
    ones = (row_iota(shape) // HD == lane_iota(shape) // HD).astype(BF16)

    def part(y):
        high, low = split(y)
        return jnp.dot(high.astype(BF16), ones, preferred_element_type=F32) + jnp.dot(
            low.astype(BF16), ones, preferred_element_type=F32
        )

    return by_lanes(part, x)


def rope(x, cosine, sine):
    first = (lane_iota((ROWS, LANES)) % HD) < (HD // 2)

    def part(y):
        other = jnp.where(
            first, pltpu.roll(y, LANES - HD // 2, 1), pltpu.roll(y, HD // 2, 1)
        )
        return y * cosine + other * sine

    return by_lanes(part, x)


def front_kernel(
    hist_hbm,
    inv_hbm,
    ngain_hbm,
    decay_hbm,
    hgain_hbm,
    mgain_hbm,
    group_hbm,
    inner_hbm,
    weight_hbm,
    tok_hbm,
    wq_hbm,
    wk_hbm,
    wv_hbm,
    wg_hbm,
    state_hbm,
    wo_hbm,
    mixed_ref,
    send_ref,
    k_ref,
    v_ref,
    slot_ref,
    weight_ref,
    hist,
    inv,
    ngain,
    decay,
    hgain,
    mgain,
    group,
    inner,
    seen,
    tok,
    w4,
    wo,
    st,
    qs,
    part,
    wide,
    scales,
    small_sem,
    w_sem,
    st_sem,
):
    small = [
        pltpu.make_async_copy(src, dst, small_sem.at[i])
        for i, (src, dst) in enumerate(
            (
                (tok_hbm, tok),
                (ngain_hbm, ngain),
                (hist_hbm, hist),
                (inv_hbm, inv),
                (decay_hbm, decay),
                (hgain_hbm, hgain),
                (mgain_hbm, mgain),
                (group_hbm, group),
                (inner_hbm, inner),
                (weight_hbm, weight_ref),
            )
        )
    ]
    weights = [
        pltpu.make_async_copy(src, w4.at[i], w_sem.at[i])
        for i, src in enumerate((wq_hbm, wk_hbm, wv_hbm, wg_hbm))
    ]
    wo_copy = pltpu.make_async_copy(wo_hbm, wo, w_sem.at[4])

    def state_copy(i):
        rows = pl.ds(i * GROUP, GROUP)
        return pltpu.make_async_copy(state_hbm.at[rows], st.at[rows], st_sem.at[i])

    for copy in small:
        copy.start()
    for copy in weights:
        copy.start()
    for copy in small:
        copy.wait()
    state_copy(0).start()

    x = tok[...].astype(F32)
    scale = lax.rsqrt(jnp.mean(x * x, axis=-1, keepdims=True) + EPS)
    normed = (x * scale * ngain[...]).astype(BF16)

    square = (ROWS, ROWS)
    place = jnp.sum(
        jnp.where(
            row_iota(square) == lane_iota(square),
            jnp.broadcast_to(hist[...].astype(F32), square),
            0.0,
        ),
        axis=1,
        keepdims=True,
    )
    angles = place * inv[...]
    cosine = jnp.cos(angles)
    sine = jnp.sin(angles)
    sine = jnp.where((lane_iota((ROWS, LANES)) % HD) < (HD // 2), -sine, sine)

    for e in range(EXPERTS):
        seen[e] = 0
    for t in range(ROWS):
        for j in range(2):
            e = group[t] * PER_GROUP + inner[j, t]
            slot = seen[e]
            seen[e] = 1
            slot_ref[j, t] = 2 * e + slot
    zero = jnp.zeros((TILES, LANES), BF16)
    for e in range(2 * EXPERTS):
        send_ref[e] = zero

    def project(i):
        weights[i].wait()
        return jnp.dot(normed, w4[i], preferred_element_type=F32).astype(BF16).astype(F32)

    q = project(0)
    for i in range(1, 3):
        state_copy(i).start()
    q = rope(q, cosine, sine)
    k = project(1)
    for i in range(3, CHUNKS):
        state_copy(i).start()
    wo_copy.start()
    k = rope(k, cosine, sine) * (HD**-0.5)
    v = project(2)
    gate = project(3)
    for i, piece in enumerate(split(q)):
        qs[i] = piece
    k_ref[...] = k
    v_ref[...] = v

    fresh = head_sum(q * k) * v
    heads = lane_iota((1, RW)) // HD
    rate = jnp.zeros((1, RW), F32)
    for h in range(HEADS):
        rate = jnp.where(heads == h, decay[h], rate)
    retain = jnp.exp(-rate)
    own = row_iota((HEADS, RW)) == lane_iota((HEADS, RW)) // HD

    def read(t):
        spread = [
            jnp.where(own, jnp.broadcast_to(qs[s, pl.ds(t, 1), :], (HEADS, RW)), 0.0)
            for s in range(2)
        ]
        total = jnp.dot(
            jnp.concatenate(spread, axis=0).astype(BF16),
            st[t].reshape(RW, HD).astype(BF16),
            preferred_element_type=F32,
        )
        part[pl.ds(pl.multiple_of(t * HEADS, HEADS), HEADS), 0:HD] = (
            total[0:HEADS] + total[HEADS:]
        )

    def chunk(i, carry):
        state_copy(i).wait()
        for b in range(GROUP):
            read(i * GROUP + b)
        return carry

    lax.fori_loop(0, CHUNKS, chunk, 0)

    def head_rows(h):
        return part[pl.ds(h, ROWS, stride=HEADS), :]

    low_half = lane_iota((ROWS, LANES)) < HD
    old = jnp.concatenate(
        [
            jnp.where(
                low_half, head_rows(2 * c), pltpu.roll(head_rows(2 * c + 1), HD, 1)
            )
            for c in range(HEADS // 2)
        ],
        axis=1,
    )
    reading = retain * old + fresh
    mean_square = head_sum(reading * reading) * (1.0 / HD)
    reading = reading * lax.rsqrt(mean_square + EPS) * hgain[...]
    mixed_heads = (reading * jax.nn.silu(gate)).astype(BF16)
    wo_copy.wait()
    squares = jnp.zeros((ROWS, LANES), F32)
    for n in range(0, D, 2 * LANES):
        block = slice(n, n + 2 * LANES)
        mixed = tok[:, block].astype(F32) + jnp.dot(
            mixed_heads, wo[:, block], preferred_element_type=F32
        )
        mixed = mixed.astype(BF16).astype(F32)
        for i in range(2):
            piece = mixed[:, i * LANES : (i + 1) * LANES]
            squares = squares + piece * piece
            wide[pl.ds(n // LANES + i, ROWS, stride=TILES), :] = piece
    scale = lax.rsqrt(jnp.sum(squares, axis=-1, keepdims=True) * (1.0 / D) + EPS)
    scales[...] = jnp.broadcast_to(scale, (ROWS, LANES))
    for t in range(ROWS):
        tile = wide[t * TILES : (t + 1) * TILES, :]
        mixed_ref[t] = tile.astype(BF16)
        row = (tile * scales[t : t + 1, :] * mgain[...]).astype(BF16)
        for j in range(2):
            send_ref[slot_ref[j, t]] = row


def state_kernel(decay, state_ref, k_ref, v_ref, new_ref):
    k = k_ref[...]
    high = k.astype(BF16).astype(F32)
    kt = jnp.concatenate([high, k - high], axis=0).T.astype(BF16)
    v = v_ref[...]
    swapped = jnp.concatenate(
        [
            pltpu.roll(v[:, c * LANES : (c + 1) * LANES], HD, 1)
            for c in range(RW // LANES)
        ],
        axis=1,
    )
    retains = [jnp.exp(jnp.full((HD, HD), -decay[h], F32)) for h in range(HEADS)]
    for pair in range(GROUP // 2):
        shape = (2 * GROUP, 2 * LANES)
        pick = (
            lax.broadcasted_iota(jnp.int32, shape, 0) % GROUP
            == lane_iota(shape) // LANES + 2 * pair
        ).astype(BF16)
        columns = jnp.dot(kt, pick, preferred_element_type=F32)
        for i in range(2):
            b = 2 * pair + i
            for h in range(HEADS):
                column = columns[h * HD : (h + 1) * HD, i * LANES : i * LANES + HD]
                c = (h // 2) * LANES
                row = (swapped if h % 2 else v)[b : b + 1, c : c + HD]
                new_ref[b, h] = retains[h] * state_ref[b, h] + column * row


def expert_kernel(
    in_ref, wg_ref, wu_ref, wd_hbm, out_hbm, wide, lhs, out, down, sem, down_sem
):
    down_copy = pltpu.make_async_copy(wd_hbm, down, down_sem)
    down_copy.start()
    copies = []
    for i in range(2 * EXPERTS // BLOCK):
        rows = pl.ds(i * BLOCK, BLOCK)
        wide[i] = in_ref[rows].astype(F32).reshape(BLOCK * TILES, LANES)
        for r in range(TILES):
            lhs[rows, r * LANES : (r + 1) * LANES] = wide[
                i, pl.ds(r, BLOCK, stride=TILES), :
            ].astype(BF16)
        gate = jnp.dot(lhs[rows], wg_ref[0], preferred_element_type=F32)
        up = jnp.dot(lhs[rows], wu_ref[0], preferred_element_type=F32)
        hidden = (jax.nn.silu(gate) * up).astype(BF16)
        if i == 0:
            down_copy.wait()
        result = jnp.dot(hidden, down[0], preferred_element_type=F32)
        for r in range(TILES):
            wide[i, pl.ds(r, BLOCK, stride=TILES), :] = result[
                :, r * LANES : (r + 1) * LANES
            ]
        out[rows] = wide[i].astype(BF16).reshape(BLOCK, TILES, LANES)
        copy = pltpu.make_async_copy(out.at[rows], out_hbm.at[rows], sem.at[i])
        copy.start()
        copies.append(copy)
    for copy in copies:
        copy.wait()


def combine_kernel(slot, weight, mixed_ref, back_ref, out_hbm, wide, out, sem):
    copies = []
    for i in range(ROWS // PART):
        for t in range(i * PART, (i + 1) * PART):
            total = mixed_ref[t].astype(F32)
            for j in range(2):
                total = total + back_ref[slot[j, t]].astype(F32) * weight[j, t]
            wide[t * TILES : (t + 1) * TILES, :] = total
        rows = pl.ds(i * PART, PART)
        for r in range(TILES):
            out[rows, r * LANES : (r + 1) * LANES] = wide[
                pl.ds(i * PART * TILES + r, PART, stride=TILES), :
            ].astype(BF16)
        copy = pltpu.make_async_copy(out.at[rows], out_hbm.at[rows], sem.at[i])
        copy.start()
        copies.append(copy)
    for copy in copies:
        copy.wait()


def in_vmem(x):
    return pltpu.with_memory_space_constraint(x, pltpu.VMEM)


def in_smem(x):
    return pltpu.with_memory_space_constraint(x, pltpu.SMEM)


def in_hbm(x):
    return pltpu.with_memory_space_constraint(x, pltpu.HBM)


HBM = pl.BlockSpec(memory_space=pltpu.HBM)
VMEM = pl.BlockSpec(memory_space=pltpu.VMEM)
SMEM = pl.BlockSpec(memory_space=pltpu.SMEM)
ROW_TILES = (2 * EXPERTS, TILES, LANES)


def local(
    tokens,
    history_length,
    norm_gain,
    w_query,
    w_key,
    w_value,
    w_gate,
    decay_rate,
    state,
    head_gain,
    w_out,
    moe_gain,
    route_weights,
    expert_group,
    expert_inner,
    expert_gate,
    expert_up,
    expert_down,
):
    inner = expert_inner.T
    inverse = jnp.asarray(
        (10000.0 ** (-(np.arange(LANES) % 32) / 32.0)).astype(np.float32).reshape(1, LANES)
    )
    mixed, send, keys, values, slots, weights = pl.pallas_call(
        front_kernel,
        out_shape=[
            pltpu.VMEM((ROWS, TILES, LANES), BF16),
            pltpu.VMEM(ROW_TILES, BF16),
            pltpu.VMEM((ROWS, RW), F32),
            pltpu.VMEM((ROWS, RW), F32),
            pltpu.SMEM((2, ROWS), jnp.int32),
            pltpu.SMEM((2, ROWS), F32),
        ],
        in_specs=[HBM] * 16,
        out_specs=[VMEM, VMEM, VMEM, VMEM, SMEM, SMEM],
        scratch_shapes=[
            pltpu.VMEM((1, ROWS), jnp.int32),
            pltpu.VMEM((1, LANES), F32),
            pltpu.VMEM((1, D), F32),
            pltpu.SMEM((HEADS,), F32),
            pltpu.VMEM((1, RW), F32),
            pltpu.VMEM((TILES, LANES), F32),
            pltpu.SMEM((ROWS,), jnp.int32),
            pltpu.SMEM((2, ROWS), jnp.int32),
            pltpu.SMEM((EXPERTS,), jnp.int32),
            pltpu.VMEM((ROWS, D), BF16),
            pltpu.VMEM((4, D, RW), BF16),
            pltpu.VMEM((RW, D), BF16),
            pltpu.VMEM((ROWS, HEADS, HD, HD), F32),
            pltpu.VMEM((2, ROWS, RW), F32),
            pltpu.VMEM((HEADS * ROWS, LANES), F32),
            pltpu.VMEM((ROWS * TILES, LANES), F32),
            pltpu.VMEM((ROWS, LANES), F32),
            pltpu.SemaphoreType.DMA((10,)),
            pltpu.SemaphoreType.DMA((5,)),
            pltpu.SemaphoreType.DMA((CHUNKS,)),
        ],
        compiler_params=pltpu.CompilerParams(vmem_limit_bytes=32 * 2**20),
        name="front",
    )(
        *(
            in_hbm(x)
            for x in (
                history_length.reshape(1, ROWS),
                inverse,
                norm_gain.reshape(1, D),
                decay_rate,
                head_gain.reshape(1, RW),
                moe_gain.reshape(TILES, LANES),
                expert_group,
                inner,
                route_weights.T,
                tokens,
                w_query,
                w_key,
                w_value,
                w_gate,
                state,
                w_out,
            )
        )
    )

    new_state = pl.pallas_call(
        state_kernel,
        grid=(CHUNKS,),
        out_shape=jax.ShapeDtypeStruct(state.shape, F32),
        in_specs=[
            SMEM,
            pl.BlockSpec((GROUP, HEADS, HD, HD), lambda i: (i, 0, 0, 0)),
            pl.BlockSpec((GROUP, RW), lambda i: (i, 0)),
            pl.BlockSpec((GROUP, RW), lambda i: (i, 0)),
        ],
        out_specs=pl.BlockSpec((GROUP, HEADS, HD, HD), lambda i: (i, 0, 0, 0)),
        cost_estimate=pl.CostEstimate(
            flops=10**9, bytes_accessed=26 * 10**6, transcendentals=0
        ),
        compiler_params=pltpu.CompilerParams(vmem_limit_bytes=20 * 2**20),
        name="state_update",
    )(in_hbm(decay_rate), in_hbm(state), in_vmem(keys), in_vmem(values))

    def dispatch(rows):
        return lax.all_to_all(rows, "ep", split_axis=0, concat_axis=0, tiled=True)

    outputs = pl.pallas_call(
        expert_kernel,
        out_shape=jax.ShapeDtypeStruct(ROW_TILES, BF16),
        in_specs=[VMEM, VMEM, VMEM, HBM],
        out_specs=HBM,
        scratch_shapes=[
            pltpu.VMEM((2 * EXPERTS // BLOCK, BLOCK * TILES, LANES), F32),
            pltpu.VMEM((2 * EXPERTS, D), BF16),
            pltpu.VMEM(ROW_TILES, BF16),
            pltpu.VMEM((1, RW // 2, D), BF16),
            pltpu.SemaphoreType.DMA((2 * EXPERTS // BLOCK,)),
            pltpu.SemaphoreType.DMA,
        ],
        cost_estimate=pl.CostEstimate(
            flops=8 * 10**8, bytes_accessed=4 * 10**6, transcendentals=0
        ),
        compiler_params=pltpu.CompilerParams(vmem_limit_bytes=16 * 2**20),
        name="expert",
    )(
        in_vmem(dispatch(send)),
        in_vmem(expert_gate),
        in_vmem(expert_up),
        in_hbm(expert_down),
    )
    output = pl.pallas_call(
        combine_kernel,
        out_shape=jax.ShapeDtypeStruct((ROWS, D), BF16),
        in_specs=[SMEM, SMEM, VMEM, VMEM],
        out_specs=HBM,
        scratch_shapes=[
            pltpu.VMEM((ROWS * TILES, LANES), F32),
            pltpu.VMEM((ROWS, D), BF16),
            pltpu.SemaphoreType.DMA((ROWS // PART,)),
        ],
        compiler_params=pltpu.CompilerParams(vmem_limit_bytes=8 * 2**20),
        name="combine",
    )(in_smem(slots), in_smem(weights), in_vmem(mixed), in_vmem(dispatch(outputs)))
    return output, new_state


def solution(mesh):
    return jax.shard_map(
        local,
        mesh=mesh,
        in_specs=(
            P("ep", None),
            P("ep"),
            P(),
            P(),
            P(),
            P(),
            P(),
            P(),
            P("ep", None, None, None),
            P(),
            P(),
            P(),
            P("ep", None),
            P("ep"),
            P("ep", None),
            P("ep", None, None),
            P("ep", None, None),
            P("ep", None, None),
        ),
        out_specs=(P("ep", None), P("ep", None, None, None)),
        check_vma=False,
    )
```

time: 69.6 us -> 68.7 us (0.987)
  Pallas kernels: 27.1 us -> 24.8 us
  waiting for transfers between devices: 6.61 us -> 7.96 us
    all_to_all x1, waiting for transfers between devices: 6.61 us -> 7.96 us  [dispatch(): return lax.all_to_all(rows, 'ep', split_axis=0, concat_axis=0, tiled=True)]
    pallas_call x1, Pallas kernels: 9.74 us -> 8.91 us  [local(): pl.pallas_call(front_kernel, out_shape=[pltpu.VMEM((ROWS, TILES, LANES),...]
    pallas_call x1, Pallas kernels: 1.62 us -> 0.87 us  [local(): pl.pallas_call(combine_kernel, out_shape=jax.ShapeDtypeStruct((ROWS, D),...]
  transfers between devices with their start and end apart: 1 -> 1, of which waited for: 1 -> 1; matrix products, arithmetic and copies ran while one was open for 0% -> 0% of each run, Pallas kernels for 18% -> 17%
where the time goes in v3:
time: 68.7 us; the launch traced here: 68.4 us
  blocking collectives  30.5 us (44%)
  Pallas kernels  24.8 us (36%)
  waiting for transfers between devices  7.96 us (12%)
  starting transfers between devices  4.43 us (6%)
    all_to_all x1, blocking collectives, dispatch(): return lax.all_to_all(rows, 'ep', split_axis=0, concat_axis=0, tiled=True)  30.5 us
    pallas_call x1, Pallas kernels, local(): pl.pallas_call(state_kernel, grid=(CHUNKS,), out_shape=jax.ShapeDtypeStru...  11.4 us
    pallas_call x1, Pallas kernels, local(): pl.pallas_call(front_kernel, out_shape=[pltpu.VMEM((ROWS, TILES, LANES),...  8.91 us
    all_to_all x1, waiting for transfers between devices, dispatch(): return lax.all_to_all(rows, 'ep', split_axis=0, concat_axis=0, tiled=True)  7.96 us
    all_to_all x1, starting transfers between devices, dispatch(): return lax.all_to_all(rows, 'ep', split_axis=0, concat_axis=0, tiled=True)  4.43 us
    pallas_call x1, Pallas kernels, local(): pl.pallas_call(expert_kernel, out_shape=jax.ShapeDtypeStruct(ROW_TILES, B...  3.67 us
  transfers between devices with their start and end apart: 1, of which 1 were waited for; matrix products, arithmetic and copies ran while one was open for 0% of the time, Pallas kernels for 17%

profile of v3, /device:TPU:1, one launch (start us, length us, event | category | flops | bytes accessed | tf_op | source)
XLA Modules:
  0.0 68.4 jit_solution(11086245778001941499)
XLA Ops:
  0.6 8.9 %front.1 = (bf16[48,16,128]{2,1,0:T(8,128)(2,1)S(1)}, bf16[256,16,128]{2,1,0:T(8,128)(2,1)S(1)}, f32[48,512]{1,0:T(8,128)S(1)}, f32[48,512]{1,0:T(8,128)S(1)}, s32[2,48]{1,0:T(2,128)S(4)}, /*index=5*/f32[2,48]{1,0:T(2,128)S(4)}) custom-call(s32[1,48]{1,0:T(1,128)} %bitcast.11, f32[1,128]{1,0:T(1,128)} %constant.2.clone.inv_hbm, f32[1,2048]{1,0:T(1,128)} %bitcast.6, ...), custom_call_target="tpu_custom_call" | custom-call | tf_op jit(solution)/shard_map/front/pallas_call | solution.py:395
  9.6 0.0 copy-start
  9.6 0.0 copy-start.1
  9.6 30.5 %all_to_all.10.in_ref = bf16[256,16,128]{2,1,0:T(8,128)(2,1)S(1)} all-to-all(bf16[256,16,128]{2,1,0:T(8,128)(2,1)S(1)} %get-tuple-element.11), channel_id=1, replica_groups=mesh['ep'=128] {'ep'}, dimensions={0} | all-to-all | bytes 2097152 | tf_op jit(solution)/shard_map/all_to_all | solution.py:474
  40.1 0.0 copy-done
  40.1 0.0 copy-done.1
  40.1 3.7 %expert.1 = bf16[256,16,128]{2,1,0:T(8,128)(2,1)} custom-call(bf16[256,16,128]{2,1,0:T(8,128)(2,1)S(1)} %all_to_all.10.in_ref, bf16[1,2048,256]{2,1,0:T(8,128)(2,1)S(1)} %copy-done, bf16[1,2048,256]{2,1,0:T(8,128)(2,1)S(1)} %copy-done.1, bf16[1,256,2048]{2,1,0:T(8,128)(2,1)} %wd_hbm.1), custom_call_target="tpu_custom_call" | custom-call | flops 800000000 | bytes 4000000 | tf_op jit(solution)/shard_map/expert/pallas_call | solution.py:476
  43.8 4.4 %all-to-all-start.1 = ((bf16[256,16,128]{2,1,0:T(8,128)(2,1)}), bf16[256,16,128]{2,1,0:T(8,128)(2,1)S(1)}, u32[]{:S(2)}, u32[]{:S(2)}) async-start(bf16[256,16,128]{2,1,0:T(8,128)(2,1)} %expert.1), calls=%async_computation.1 | async-start | bytes 2097152 | tf_op jit(solution)/shard_map/all_to_all | solution.py:474
  48.2 11.4 %state_update.1 = f32[48,8,64,64]{3,2,1,0:T(8,128)} custom-call(f32[8]{0:T(128)} %decay.1, f32[48,8,64,64]{3,2,1,0:T(8,128)} %state_ref.1, f32[48,512]{1,0:T(8,128)S(1)} %get-tuple-element.12.k_ref, f32[48,512]{1,0:T(8,128)S(1)} %get-tuple-element.13.v_ref), custom_call_target="tpu_custom_call" | custom-call | flops 1000000000 | bytes 26000000 | tf_op jit(solution)/shard_map/state_update/pallas_call | solution.py:455
  59.6 8.0 %all-to-all-done.1.back_ref = bf16[256,16,128]{2,1,0:T(8,128)(2,1)S(1)} async-done(((bf16[256,16,128]{2,1,0:T(8,128)(2,1)}), bf16[256,16,128]{2,1,0:T(8,128)(2,1)S(1)}, u32[]{:S(2)}, u32[]{:S(2)}) %all-to-all-start.1) | async-done | bytes 1048608 | tf_op jit(solution)/shard_map/all_to_all | solution.py:474
  67.6 0.9 %combine.1 = bf16[48,2048]{1,0:T(8,128)(2,1)} custom-call(s32[2,48]{1,0:T(2,128)S(4)} %get-tuple-element.8.slot, f32[2,48]{1,0:T(2,128)S(4)} %get-tuple-element.9.weight, bf16[48,16,128]{2,1,0:T(8,128)(2,1)S(1)} %get-tuple-element.10.mixed_ref, bf16[256,16,128]{2,1,0:T(8,128)(2,1)S(1)} %all-to-all-done.1.back_ref), custom_call_target="tpu_custom_call" | custom-call | tf_op jit(solution)/shard_map/combine/pallas_call | solution.py:500
Async XLA Ops:
  9.6 30.5 %copy-start = (bf16[1,2048,256]{2,1,0:T(8,128)(2,1)S(1)}, bf16[1,2048,256]{2,1,0:T(8,128)(2,1)}, u32[]{:S(2)}) copy-start(bf16[1,2048,256]{2,1,0:T(8,128)(2,1)} %wg_ref.1) | copy-start | bytes 3145732
  9.6 30.5 %copy-start.1 = (bf16[1,2048,256]{2,1,0:T(8,128)(2,1)S(1)}, bf16[1,2048,256]{2,1,0:T(8,128)(2,1)}, u32[]{:S(2)}) copy-start(bf16[1,2048,256]{2,1,0:T(8,128)(2,1)} %wu_ref.1) | copy-start | bytes 3145732
  43.8 23.8 %all-to-all-start.1 = ((bf16[256,16,128]{2,1,0:T(8,128)(2,1)}), bf16[256,16,128]{2,1,0:T(8,128)(2,1)S(1)}, u32[]{:S(2)}, u32[]{:S(2)}) async-start(bf16[256,16,128]{2,1,0:T(8,128)(2,1)} %expert.1), calls=%async_computation.1 | async-start | bytes 2097152 | tf_op jit(solution)/shard_map/all_to_all | solution.py:474

commit v4 on v3

--- a/solution.py
+++ b/solution.py
@@ -20,8 +20,9 @@
 TILES = D // LANES
 GROUP = 8
 CHUNKS = ROWS // GROUP
-BLOCK = 128
+STEP = 20
 PART = 16
+COPIES = 4
 F32 = jnp.float32
 BF16 = jnp.bfloat16
 
@@ -88,12 +89,14 @@
     wg_hbm,
     state_hbm,
     wo_hbm,
+    down_hbm,
     mixed_ref,
     send_ref,
     k_ref,
     v_ref,
     slot_ref,
     weight_ref,
+    down_ref,
     hist,
     inv,
     ngain,
@@ -137,6 +140,7 @@
         for i, src in enumerate((wq_hbm, wk_hbm, wv_hbm, wg_hbm))
     ]
     wo_copy = pltpu.make_async_copy(wo_hbm, wo, w_sem.at[4])
+    down_copy = pltpu.make_async_copy(down_hbm, down_ref, w_sem.at[5])
 
     def state_copy(i):
         rows = pl.ds(i * GROUP, GROUP)
@@ -195,6 +199,7 @@
     wo_copy.start()
     k = rope(k, cosine, sine) * (HD**-0.5)
     v = project(2)
+    down_copy.start()
     gate = project(3)
     for i, piece in enumerate(split(q)):
         qs[i] = piece
@@ -219,7 +224,7 @@
             st[t].reshape(RW, HD).astype(BF16),
             preferred_element_type=F32,
         )
-        part[pl.ds(pl.multiple_of(t * HEADS, HEADS), HEADS), 0:HD] = (
+        part[pl.ds(t * (HEADS + 1), HEADS), 0:HD] = (
             total[0:HEADS] + total[HEADS:]
         )
 
@@ -232,7 +237,7 @@
     lax.fori_loop(0, CHUNKS, chunk, 0)
 
     def head_rows(h):
-        return part[pl.ds(h, ROWS, stride=HEADS), :]
+        return part[pl.ds(h, ROWS, stride=HEADS + 1), :]
 
     low_half = lane_iota((ROWS, LANES)) < HD
     old = jnp.concatenate(
@@ -259,15 +264,16 @@
         for i in range(2):
             piece = mixed[:, i * LANES : (i + 1) * LANES]
             squares = squares + piece * piece
-            wide[pl.ds(n // LANES + i, ROWS, stride=TILES), :] = piece
+            wide[pl.ds(n // LANES + i, ROWS, stride=STEP), :] = piece
     scale = lax.rsqrt(jnp.sum(squares, axis=-1, keepdims=True) * (1.0 / D) + EPS)
     scales[...] = jnp.broadcast_to(scale, (ROWS, LANES))
     for t in range(ROWS):
-        tile = wide[t * TILES : (t + 1) * TILES, :]
+        tile = wide[t * STEP : t * STEP + TILES, :]
         mixed_ref[t] = tile.astype(BF16)
         row = (tile * scales[t : t + 1, :] * mgain[...]).astype(BF16)
         for j in range(2):
             send_ref[slot_ref[j, t]] = row
+    down_copy.wait()
 
 
 def state_kernel(decay, state_ref, k_ref, v_ref, new_ref):
@@ -299,31 +305,25 @@
                 new_ref[b, h] = retains[h] * state_ref[b, h] + column * row
 
 
-def expert_kernel(
-    in_ref, wg_ref, wu_ref, wd_hbm, out_hbm, wide, lhs, out, down, sem, down_sem
-):
-    down_copy = pltpu.make_async_copy(wd_hbm, down, down_sem)
-    down_copy.start()
+def expert_kernel(in_ref, wg_ref, wu_ref, wd_ref, out_hbm, wide, lhs, out, sem):
+    n = 2 * EXPERTS
+    for i in range(n):
+        wide[i * STEP : i * STEP + TILES, :] = in_ref[i].astype(F32)
+    for r in range(TILES):
+        lhs[:, r * LANES : (r + 1) * LANES] = wide[pl.ds(r, n, stride=STEP), :].astype(BF16)
+    rows = lhs[...]
+    gate = jnp.dot(rows, wg_ref[0], preferred_element_type=F32)
+    up = jnp.dot(rows, wu_ref[0], preferred_element_type=F32)
+    hidden = (jax.nn.silu(gate) * up).astype(BF16)
+    result = jnp.dot(hidden, wd_ref[0], preferred_element_type=F32)
+    for r in range(TILES):
+        wide[pl.ds(r, n, stride=STEP), :] = result[:, r * LANES : (r + 1) * LANES]
     copies = []
-    for i in range(2 * EXPERTS // BLOCK):
-        rows = pl.ds(i * BLOCK, BLOCK)
-        wide[i] = in_ref[rows].astype(F32).reshape(BLOCK * TILES, LANES)
-        for r in range(TILES):
-            lhs[rows, r * LANES : (r + 1) * LANES] = wide[
-                i, pl.ds(r, BLOCK, stride=TILES), :
-            ].astype(BF16)
-        gate = jnp.dot(lhs[rows], wg_ref[0], preferred_element_type=F32)
-        up = jnp.dot(lhs[rows], wu_ref[0], preferred_element_type=F32)
-        hidden = (jax.nn.silu(gate) * up).astype(BF16)
-        if i == 0:
-            down_copy.wait()
-        result = jnp.dot(hidden, down[0], preferred_element_type=F32)
-        for r in range(TILES):
-            wide[i, pl.ds(r, BLOCK, stride=TILES), :] = result[
-                :, r * LANES : (r + 1) * LANES
-            ]
-        out[rows] = wide[i].astype(BF16).reshape(BLOCK, TILES, LANES)
-        copy = pltpu.make_async_copy(out.at[rows], out_hbm.at[rows], sem.at[i])
+    for c in range(COPIES):
+        for i in range(c * n // COPIES, (c + 1) * n // COPIES):
+            out[i] = wide[i * STEP : i * STEP + TILES, :].astype(BF16)
+        rows = pl.ds(c * n // COPIES, n // COPIES)
+        copy = pltpu.make_async_copy(out.at[rows], out_hbm.at[rows], sem.at[c])
         copy.start()
         copies.append(copy)
     for copy in copies:
@@ -337,11 +337,11 @@
             total = mixed_ref[t].astype(F32)
             for j in range(2):
                 total = total + back_ref[slot[j, t]].astype(F32) * weight[j, t]
-            wide[t * TILES : (t + 1) * TILES, :] = total
+            wide[t * STEP : t * STEP + TILES, :] = total
         rows = pl.ds(i * PART, PART)
         for r in range(TILES):
             out[rows, r * LANES : (r + 1) * LANES] = wide[
-                pl.ds(i * PART * TILES + r, PART, stride=TILES), :
+                pl.ds(i * PART * STEP + r, PART, stride=STEP), :
             ].astype(BF16)
         copy = pltpu.make_async_copy(out.at[rows], out_hbm.at[rows], sem.at[i])
         copy.start()
@@ -392,7 +392,7 @@
     inverse = jnp.asarray(
         (10000.0 ** (-(np.arange(LANES) % 32) / 32.0)).astype(np.float32).reshape(1, LANES)
     )
-    mixed, send, keys, values, slots, weights = pl.pallas_call(
+    mixed, send, keys, values, slots, weights, down = pl.pallas_call(
         front_kernel,
         out_shape=[
             pltpu.VMEM((ROWS, TILES, LANES), BF16),
@@ -401,9 +401,10 @@
             pltpu.VMEM((ROWS, RW), F32),
             pltpu.SMEM((2, ROWS), jnp.int32),
             pltpu.SMEM((2, ROWS), F32),
-        ],
-        in_specs=[HBM] * 16,
-        out_specs=[VMEM, VMEM, VMEM, VMEM, SMEM, SMEM],
+            pltpu.VMEM(expert_down.shape, BF16),
+        ],
+        in_specs=[HBM] * 17,
+        out_specs=[VMEM, VMEM, VMEM, VMEM, SMEM, SMEM, VMEM],
         scratch_shapes=[
             pltpu.VMEM((1, ROWS), jnp.int32),
             pltpu.VMEM((1, LANES), F32),
@@ -419,11 +420,11 @@
             pltpu.VMEM((RW, D), BF16),
             pltpu.VMEM((ROWS, HEADS, HD, HD), F32),
             pltpu.VMEM((2, ROWS, RW), F32),
-            pltpu.VMEM((HEADS * ROWS, LANES), F32),
-            pltpu.VMEM((ROWS * TILES, LANES), F32),
+            pltpu.VMEM(((HEADS + 1) * ROWS, LANES), F32),
+            pltpu.VMEM((ROWS * STEP, LANES), F32),
             pltpu.VMEM((ROWS, LANES), F32),
             pltpu.SemaphoreType.DMA((10,)),
-            pltpu.SemaphoreType.DMA((5,)),
+            pltpu.SemaphoreType.DMA((6,)),
             pltpu.SemaphoreType.DMA((CHUNKS,)),
         ],
         compiler_params=pltpu.CompilerParams(vmem_limit_bytes=32 * 2**20),
@@ -448,6 +449,7 @@
                 w_gate,
                 state,
                 w_out,
+                expert_down,
             )
         )
     )
@@ -476,15 +478,13 @@
     outputs = pl.pallas_call(
         expert_kernel,
         out_shape=jax.ShapeDtypeStruct(ROW_TILES, BF16),
-        in_specs=[VMEM, VMEM, VMEM, HBM],
+        in_specs=[VMEM] * 4,
         out_specs=HBM,
         scratch_shapes=[
-            pltpu.VMEM((2 * EXPERTS // BLOCK, BLOCK * TILES, LANES), F32),
+            pltpu.VMEM((2 * EXPERTS * STEP, LANES), F32),
             pltpu.VMEM((2 * EXPERTS, D), BF16),
             pltpu.VMEM(ROW_TILES, BF16),
-            pltpu.VMEM((1, RW // 2, D), BF16),
-            pltpu.SemaphoreType.DMA((2 * EXPERTS // BLOCK,)),
-            pltpu.SemaphoreType.DMA,
+            pltpu.SemaphoreType.DMA((COPIES,)),
         ],
         cost_estimate=pl.CostEstimate(
             flops=8 * 10**8, bytes_accessed=4 * 10**6, transcendentals=0
@@ -495,7 +495,7 @@
         in_vmem(dispatch(send)),
         in_vmem(expert_gate),
         in_vmem(expert_up),
-        in_hbm(expert_down),
+        in_vmem(down),
     )
     output = pl.pallas_call(
         combine_kernel,
@@ -503,7 +503,7 @@
         in_specs=[SMEM, SMEM, VMEM, VMEM],
         out_specs=HBM,
         scratch_shapes=[
-            pltpu.VMEM((ROWS * TILES, LANES), F32),
+            pltpu.VMEM((ROWS * STEP, LANES), F32),
             pltpu.VMEM((ROWS, D), BF16),
             pltpu.SemaphoreType.DMA((ROWS // PART,)),
         ],

time: 68.7 us -> 67.1 us (0.977)
  Pallas kernels: 24.8 us -> 23.2 us
    pallas_call x1, Pallas kernels: 3.67 us -> 2.16 us  [local(): pl.pallas_call(expert_kernel, out_shape=jax.ShapeDtypeStruct(ROW_TILES, B...]
where the time goes in v4:
time: 67.1 us; the launch traced here: 66.8 us
  blocking collectives  30.5 us (45%)
  Pallas kernels  23.2 us (35%)
  waiting for transfers between devices  7.96 us (12%)
  starting transfers between devices  4.43 us (7%)
  between operations  0.68 us (1%)
    all_to_all x1, blocking collectives, dispatch(): return lax.all_to_all(rows, 'ep', split_axis=0, concat_axis=0, tiled=True)  30.5 us
    pallas_call x1, Pallas kernels, local(): pl.pallas_call(state_kernel, grid=(CHUNKS,), out_shape=jax.ShapeDtypeStru...  11.4 us
    pallas_call x1, Pallas kernels, local(): pl.pallas_call(front_kernel, out_shape=[pltpu.VMEM((ROWS, TILES, LANES),...  8.89 us
    all_to_all x1, waiting for transfers between devices, dispatch(): return lax.all_to_all(rows, 'ep', split_axis=0, concat_axis=0, tiled=True)  7.96 us
    all_to_all x1, starting transfers between devices, dispatch(): return lax.all_to_all(rows, 'ep', split_axis=0, concat_axis=0, tiled=True)  4.43 us
    pallas_call x1, Pallas kernels, local(): pl.pallas_call(expert_kernel, out_shape=jax.ShapeDtypeStruct(ROW_TILES, B...  2.16 us
  transfers between devices with their start and end apart: 1, of which 1 were waited for; matrix products, arithmetic and copies ran while one was open for 0% of the time, Pallas kernels for 17%

profile of v4, /device:TPU:1, one launch (start us, length us, event | category | flops | bytes accessed | tf_op | source)
XLA Modules:
  0.0 66.8 jit_solution(15041353910260459452)
XLA Ops:
  0.6 8.9 %front.1 = (bf16[48,16,128]{2,1,0:T(8,128)(2,1)S(1)}, bf16[256,16,128]{2,1,0:T(8,128)(2,1)S(1)}, f32[48,512]{1,0:T(8,128)S(1)}, f32[48,512]{1,0:T(8,128)S(1)}, s...) custom-call(s32[1,48]{1,0:T(1,128)} %bitcast.11, f32[1,128]{1,0:T(1,128)} %constant.2.clone.inv_hbm, ...), custom_call_target="tpu_custom_call" | custom-call | tf_op jit(solution)/shard_map/front/pallas_call | solution.py:395
  9.5 0.0 copy-start
  9.5 0.0 copy-start.1
  9.6 30.5 %all_to_all.10.in_ref = bf16[256,16,128]{2,1,0:T(8,128)(2,1)S(1)} all-to-all(bf16[256,16,128]{2,1,0:T(8,128)(2,1)S(1)} %get-tuple-element.12), channel_id=1, replica_groups=mesh['ep'=128] {'ep'}, dimensions={0} | all-to-all | bytes 2097152 | tf_op jit(solution)/shard_map/all_to_all | solution.py:476
  40.1 0.0 copy-done
  40.1 0.0 copy-done.1
  40.1 2.2 %expert.1 = bf16[256,16,128]{2,1,0:T(8,128)(2,1)} custom-call(bf16[256,16,128]{2,1,0:T(8,128)(2,1)S(1)} %all_to_all.10.in_ref, bf16[1,2048,256]{2,1,0:T(8,128)(2,1)S(1)} %copy-done, bf16[1,2048,256]{2,1,0:T(8,128)(2,1)S(1)} %copy-done.1, bf16[1,256,2048]{2,1,0:T(8,128)(2,1)S(1)} %get-tuple-element.13.wd_ref), custom_call_target="tpu_custom_call" | custom-call | flops 800000000 | bytes 4000000 | tf_op jit(solution)/shard_map/expert/pallas_call | solution.py:478
  42.3 4.4 %all-to-all-start.1 = ((bf16[256,16,128]{2,1,0:T(8,128)(2,1)}), bf16[256,16,128]{2,1,0:T(8,128)(2,1)S(1)}, u32[]{:S(2)}, u32[]{:S(2)}) async-start(bf16[256,16,128]{2,1,0:T(8,128)(2,1)} %expert.1), calls=%async_computation.1 | async-start | bytes 2097152 | tf_op jit(solution)/shard_map/all_to_all | solution.py:476
  46.7 11.4 %state_update.1 = f32[48,8,64,64]{3,2,1,0:T(8,128)} custom-call(f32[8]{0:T(128)} %decay.1, f32[48,8,64,64]{3,2,1,0:T(8,128)} %state_ref.1, f32[48,512]{1,0:T(8,128)S(1)} %get-tuple-element.14.k_ref, f32[48,512]{1,0:T(8,128)S(1)} %get-tuple-element.15.v_ref), custom_call_target="tpu_custom_call" | custom-call | flops 1000000000 | bytes 26000000 | tf_op jit(solution)/shard_map/state_update/pallas_call | solution.py:457
  58.1 8.0 %all-to-all-done.1.back_ref = bf16[256,16,128]{2,1,0:T(8,128)(2,1)S(1)} async-done(((bf16[256,16,128]{2,1,0:T(8,128)(2,1)}), bf16[256,16,128]{2,1,0:T(8,128)(2,1)S(1)}, u32[]{:S(2)}, u32[]{:S(2)}) %all-to-all-start.1) | async-done | bytes 1048608 | tf_op jit(solution)/shard_map/all_to_all | solution.py:476
  66.0 0.8 %combine.1 = bf16[48,2048]{1,0:T(8,128)(2,1)} custom-call(s32[2,48]{1,0:T(2,128)S(4)} %get-tuple-element.9.slot, f32[2,48]{1,0:T(2,128)S(4)} %get-tuple-element.10.weight, bf16[48,16,128]{2,1,0:T(8,128)(2,1)S(1)} %get-tuple-element.11.mixed_ref, bf16[256,16,128]{2,1,0:T(8,128)(2,1)S(1)} %all-to-all-done.1.back_ref), custom_call_target="tpu_custom_call" | custom-call | tf_op jit(solution)/shard_map/combine/pallas_call | solution.py:500
Async XLA Ops:
  9.5 30.5 %copy-start = (bf16[1,2048,256]{2,1,0:T(8,128)(2,1)S(1)}, bf16[1,2048,256]{2,1,0:T(8,128)(2,1)}, u32[]{:S(2)}) copy-start(bf16[1,2048,256]{2,1,0:T(8,128)(2,1)} %wg_ref.1) | copy-start | bytes 3145732
  9.5 30.5 %copy-start.1 = (bf16[1,2048,256]{2,1,0:T(8,128)(2,1)S(1)}, bf16[1,2048,256]{2,1,0:T(8,128)(2,1)}, u32[]{:S(2)}) copy-start(bf16[1,2048,256]{2,1,0:T(8,128)(2,1)} %wu_ref.1) | copy-start | bytes 3145732
  42.3 23.8 %all-to-all-start.1 = ((bf16[256,16,128]{2,1,0:T(8,128)(2,1)}), bf16[256,16,128]{2,1,0:T(8,128)(2,1)S(1)}, u32[]{:S(2)}, u32[]{:S(2)}) async-start(bf16[256,16,128]{2,1,0:T(8,128)(2,1)} %expert.1), calls=%async_computation.1 | async-start | bytes 2097152 | tf_op jit(solution)/shard_map/all_to_all | solution.py:476

commit v5 on v4

--- a/solution.py
+++ b/solution.py
@@ -15,7 +15,6 @@
 HD = 64
 RW = HEADS * HD
 EXPERTS = 128
-PER_GROUP = 32
 LANES = 128
 TILES = D // LANES
 GROUP = 8
@@ -25,6 +24,15 @@
 COPIES = 4
 F32 = jnp.float32
 BF16 = jnp.bfloat16
+
+
+ORDER = [
+    (p % 4) * 32 + (p // 4 % 4) * 8 + (p // 16 % 4) * 2 + p // 64 for p in range(128)
+]
+
+
+def place_of(group, inner):
+    return group + (inner // 8) * 4 + (inner // 2 % 4) * 16 + (inner % 2) * 64
 
 
 def lane_iota(shape):
@@ -177,7 +185,7 @@
         seen[e] = 0
     for t in range(ROWS):
         for j in range(2):
-            e = group[t] * PER_GROUP + inner[j, t]
+            e = place_of(group[t], inner[j, t])
             slot = seen[e]
             seen[e] = 1
             slot_ref[j, t] = 2 * e + slot
@@ -473,7 +481,14 @@
     )(in_hbm(decay_rate), in_hbm(state), in_vmem(keys), in_vmem(values))
 
     def dispatch(rows):
-        return lax.all_to_all(rows, "ep", split_axis=0, concat_axis=0, tiled=True)
+        return lax.all_to_all(
+            rows,
+            "ep",
+            split_axis=0,
+            concat_axis=0,
+            axis_index_groups=[ORDER],
+            tiled=True,
+        )
 
     outputs = pl.pallas_call(
         expert_kernel,

time: 67.1 us -> 65.2 us (0.972)
  waiting for transfers between devices: 7.96 us -> 6.46 us
  blocking collectives: 30.5 us -> 29.1 us
  starting transfers between devices: 4.43 us -> 5.51 us
    all_to_all x1, waiting for transfers between devices: 7.96 us -> 6.46 us  [dispatch(): lax.all_to_all(rows, 'ep', split_axis=0, concat_axis=0, axis_index_groups...]
    all_to_all x1, blocking collectives: 30.5 us -> 29.1 us  [dispatch(): lax.all_to_all(rows, 'ep', split_axis=0, concat_axis=0, axis_index_groups...]
    all_to_all x1, starting transfers between devices: 4.43 us -> 5.51 us  [dispatch(): lax.all_to_all(rows, 'ep', split_axis=0, concat_axis=0, axis_index_groups...]
where the time goes in v5:
time: 65.2 us; the launch traced here: 65 us
  blocking collectives  29.1 us (45%)
  Pallas kernels  23.2 us (36%)
  waiting for transfers between devices  6.46 us (10%)
  starting transfers between devices  5.51 us (8%)
  between operations  0.68 us (1%)
    all_to_all x1, blocking collectives, dispatch(): lax.all_to_all(rows, 'ep', split_axis=0, concat_axis=0, axis_index_groups...  29.1 us
    pallas_call x1, Pallas kernels, local(): pl.pallas_call(state_kernel, grid=(CHUNKS,), out_shape=jax.ShapeDtypeStru...  11.4 us
    pallas_call x1, Pallas kernels, local(): pl.pallas_call(front_kernel, out_shape=[pltpu.VMEM((ROWS, TILES, LANES),...  8.85 us
    all_to_all x1, waiting for transfers between devices, dispatch(): lax.all_to_all(rows, 'ep', split_axis=0, concat_axis=0, axis_index_groups...  6.46 us
    all_to_all x1, starting transfers between devices, dispatch(): lax.all_to_all(rows, 'ep', split_axis=0, concat_axis=0, axis_index_groups...  5.51 us
    pallas_call x1, Pallas kernels, local(): pl.pallas_call(expert_kernel, out_shape=jax.ShapeDtypeStruct(ROW_TILES, B...  2.16 us
  transfers between devices with their start and end apart: 1, of which 1 were waited for; matrix products, arithmetic and copies ran while one was open for 0% of the time, Pallas kernels for 17%

profile of v5, /device:TPU:1, one launch (start us, length us, event | category | flops | bytes accessed | tf_op | source)
XLA Modules:
  0.0 65.0 jit_solution(4548805375417076035)
XLA Ops:
  0.6 8.8 %front.1 = (bf16[48,16,128]{2,1,0:T(8,128)(2,1)S(1)}, bf16[256,16,128]{2,1,0:T(8,128)(2,1)S(1)}, f32[48,512]{1,0:T(8,128)S(1)}, f32[48,512]{1,0:T(8,128)S(1)}, s...) custom-call(s32[1,48]{1,0:T(1,128)} %bitcast.11, f32[1,128]{1,0:T(1,128)} %constant.2.clone.inv_hbm, ...), custom_call_target="tpu_custom_call" | custom-call | tf_op jit(solution)/shard_map/front/pallas_call | solution.py:403
  9.5 0.0 copy-start
  9.5 0.0 copy-start.1
  9.5 29.1 %all_to_all.10.in_ref = bf16[256,16,128]{2,1,0:T(8,128)(2,1)S(1)} all-to-all(bf16[256,16,128]{2,1,0:T(8,128)(2,1)S(1)} %get-tuple-element.12), channel_id=1, replica_groups={{0,32,64,96,8,40,72,104,16,48,80,112,24,56,88,120,2,34,66,98,10,42,74,1..., dimensions={0} | all-to-all | bytes 2097152 | tf_op jit(solution)/shard_map/all_to_all | solution.py:484
  38.6 0.0 copy-done
  38.6 0.0 copy-done.1
  38.6 2.2 %expert.1 = bf16[256,16,128]{2,1,0:T(8,128)(2,1)} custom-call(bf16[256,16,128]{2,1,0:T(8,128)(2,1)S(1)} %all_to_all.10.in_ref, bf16[1,2048,256]{2,1,0:T(8,128)(2,1)S(1)} %copy-done, bf16[1,2048,256]{2,1,0:T(8,128)(2,1)S(1)} %copy-done.1, bf16[1,256,2048]{2,1,0:T(8,128)(2,1)S(1)} %get-tuple-element.13.wd_ref), custom_call_target="tpu_custom_call" | custom-call | flops 800000000 | bytes 4000000 | tf_op jit(solution)/shard_map/expert/pallas_call | solution.py:493
  40.8 5.5 %all-to-all-start.1 = ((bf16[256,16,128]{2,1,0:T(8,128)(2,1)}), bf16[256,16,128]{2,1,0:T(8,128)(2,1)S(1)}, u32[]{:S(2)}, u32[]{:S(2)}) async-start(bf16[256,16,128]{2,1,0:T(8,128)(2,1)} %expert.1), calls=%async_computation.1 | async-start | bytes 2097152 | tf_op jit(solution)/shard_map/all_to_all | solution.py:484
  46.3 11.4 %state_update.1 = f32[48,8,64,64]{3,2,1,0:T(8,128)} custom-call(f32[8]{0:T(128)} %decay.1, f32[48,8,64,64]{3,2,1,0:T(8,128)} %state_ref.1, f32[48,512]{1,0:T(8,128)S(1)} %get-tuple-element.14.k_ref, f32[48,512]{1,0:T(8,128)S(1)} %get-tuple-element.15.v_ref), custom_call_target="tpu_custom_call" | custom-call | flops 1000000000 | bytes 26000000 | tf_op jit(solution)/shard_map/state_update/pallas_call | solution.py:465
  57.7 6.5 %all-to-all-done.1.back_ref = bf16[256,16,128]{2,1,0:T(8,128)(2,1)S(1)} async-done(((bf16[256,16,128]{2,1,0:T(8,128)(2,1)}), bf16[256,16,128]{2,1,0:T(8,128)(2,1)S(1)}, u32[]{:S(2)}, u32[]{:S(2)}) %all-to-all-start.1) | async-done | bytes 1048608 | tf_op jit(solution)/shard_map/all_to_all | solution.py:484
  64.2 0.8 %combine.1 = bf16[48,2048]{1,0:T(8,128)(2,1)} custom-call(s32[2,48]{1,0:T(2,128)S(4)} %get-tuple-element.9.slot, f32[2,48]{1,0:T(2,128)S(4)} %get-tuple-element.10.weight, bf16[48,16,128]{2,1,0:T(8,128)(2,1)S(1)} %get-tuple-element.11.mixed_ref, bf16[256,16,128]{2,1,0:T(8,128)(2,1)S(1)} %all-to-all-done.1.back_ref), custom_call_target="tpu_custom_call" | custom-call | tf_op jit(solution)/shard_map/combine/pallas_call | solution.py:515
Async XLA Ops:
  9.5 29.1 %copy-start = (bf16[1,2048,256]{2,1,0:T(8,128)(2,1)S(1)}, bf16[1,2048,256]{2,1,0:T(8,128)(2,1)}, u32[]{:S(2)}) copy-start(bf16[1,2048,256]{2,1,0:T(8,128)(2,1)} %wg_ref.1) | copy-start | bytes 3145732
  9.5 29.1 %copy-start.1 = (bf16[1,2048,256]{2,1,0:T(8,128)(2,1)S(1)}, bf16[1,2048,256]{2,1,0:T(8,128)(2,1)}, u32[]{:S(2)}) copy-start(bf16[1,2048,256]{2,1,0:T(8,128)(2,1)} %wu_ref.1) | copy-start | bytes 3145732
  40.8 23.4 %all-to-all-start.1 = ((bf16[256,16,128]{2,1,0:T(8,128)(2,1)}), bf16[256,16,128]{2,1,0:T(8,128)(2,1)S(1)}, u32[]{:S(2)}, u32[]{:S(2)}) async-start(bf16[256,16,128]{2,1,0:T(8,128)(2,1)} %expert.1), calls=%async_computation.1 | async-start | bytes 2097152 | tf_op jit(solution)/shard_map/all_to_all | solution.py:484

commit v6 on v5

--- a/solution.py
+++ b/solution.py
@@ -26,13 +26,23 @@
 BF16 = jnp.bfloat16
 
 
-ORDER = [
-    (p % 4) * 32 + (p // 4 % 4) * 8 + (p // 16 % 4) * 2 + p // 64 for p in range(128)
+SHIFT = 21
+OUT_ORDER = [
+    ((p % 4) * 32 + (p // 4 % 4) * 8 + (p // 16 % 4) * 2 + p // 64) ^ SHIFT
+    for p in range(128)
 ]
-
-
-def place_of(group, inner):
+BACK_ORDER = [
+    (p % 4) * 32 + (p // 16 % 4) * 8 + (p // 4 % 4) * 2 + p // 64 for p in range(128)
+]
+
+
+def out_place(group, inner):
+    inner = inner ^ SHIFT
     return group + (inner // 8) * 4 + (inner // 2 % 4) * 16 + (inner % 2) * 64
+
+
+def back_place(group, inner):
+    return group + (inner // 2 % 4) * 4 + (inner // 8) * 16 + (inner % 2) * 64
 
 
 def lane_iota(shape):
@@ -114,6 +124,7 @@
     group,
     inner,
     seen,
+    target,
     tok,
     w4,
     wo,
@@ -185,10 +196,11 @@
         seen[e] = 0
     for t in range(ROWS):
         for j in range(2):
-            e = place_of(group[t], inner[j, t])
+            e = out_place(group[t], inner[j, t])
             slot = seen[e]
             seen[e] = 1
-            slot_ref[j, t] = 2 * e + slot
+            target[j, t] = 2 * e + slot
+            slot_ref[j, t] = 2 * back_place(group[t], inner[j, t]) + slot
     zero = jnp.zeros((TILES, LANES), BF16)
     for e in range(2 * EXPERTS):
         send_ref[e] = zero
@@ -280,7 +292,7 @@
         mixed_ref[t] = tile.astype(BF16)
         row = (tile * scales[t : t + 1, :] * mgain[...]).astype(BF16)
         for j in range(2):
-            send_ref[slot_ref[j, t]] = row
+            send_ref[target[j, t]] = row
     down_copy.wait()
 
 
@@ -329,7 +341,8 @@
     copies = []
     for c in range(COPIES):
         for i in range(c * n // COPIES, (c + 1) * n // COPIES):
-            out[i] = wide[i * STEP : i * STEP + TILES, :].astype(BF16)
+            k = 2 * OUT_ORDER.index(BACK_ORDER[i // 2]) + i % 2
+            out[i] = wide[k * STEP : k * STEP + TILES, :].astype(BF16)
         rows = pl.ds(c * n // COPIES, n // COPIES)
         copy = pltpu.make_async_copy(out.at[rows], out_hbm.at[rows], sem.at[c])
         copy.start()
@@ -423,6 +436,7 @@
             pltpu.SMEM((ROWS,), jnp.int32),
             pltpu.SMEM((2, ROWS), jnp.int32),
             pltpu.SMEM((EXPERTS,), jnp.int32),
+            pltpu.SMEM((2, ROWS), jnp.int32),
             pltpu.VMEM((ROWS, D), BF16),
             pltpu.VMEM((4, D, RW), BF16),
             pltpu.VMEM((RW, D), BF16),
@@ -480,13 +494,13 @@
         name="state_update",
     )(in_hbm(decay_rate), in_hbm(state), in_vmem(keys), in_vmem(values))
 
-    def dispatch(rows):
+    def exchange(rows, order):
         return lax.all_to_all(
             rows,
             "ep",
             split_axis=0,
             concat_axis=0,
-            axis_index_groups=[ORDER],
+            axis_index_groups=[order],
             tiled=True,
         )
 
@@ -507,7 +521,7 @@
         compiler_params=pltpu.CompilerParams(vmem_limit_bytes=16 * 2**20),
         name="expert",
     )(
-        in_vmem(dispatch(send)),
+        in_vmem(exchange(send, OUT_ORDER)),
         in_vmem(expert_gate),
         in_vmem(expert_up),
         in_vmem(down),
@@ -524,7 +538,7 @@
         ],
         compiler_params=pltpu.CompilerParams(vmem_limit_bytes=8 * 2**20),
         name="combine",
-    )(in_smem(slots), in_smem(weights), in_vmem(mixed), in_vmem(dispatch(outputs)))
+    )(in_smem(slots), in_smem(weights), in_vmem(mixed), in_vmem(exchange(outputs, BACK_ORDER)))
     return output, new_state
 
 

time: 65.2 us -> 65.4 us (level)
    all_to_all x1, starting transfers between devices: 5.51 us -> 4.86 us  [exchange(): lax.all_to_all(rows, 'ep', split_axis=0, concat_axis=0, axis_index_groups...]
where the time goes in v6:
time: 65.4 us; the launch traced here: 65.2 us
  blocking collectives  29.5 us (45%)
  Pallas kernels  23.8 us (36%)
  waiting for transfers between devices  6.34 us (10%)
  starting transfers between devices  4.86 us (7%)
  between operations  0.68 us (1%)
    all_to_all x1, blocking collectives, exchange(): lax.all_to_all(rows, 'ep', split_axis=0, concat_axis=0, axis_index_groups...  29.5 us
    pallas_call x1, Pallas kernels, local(): pl.pallas_call(state_kernel, grid=(CHUNKS,), out_shape=jax.ShapeDtypeStru...  11.4 us
    pallas_call x1, Pallas kernels, local(): pl.pallas_call(front_kernel, out_shape=[pltpu.VMEM((ROWS, TILES, LANES),...  9.39 us
    all_to_all x1, waiting for transfers between devices, exchange(): lax.all_to_all(rows, 'ep', split_axis=0, concat_axis=0, axis_index_groups...  6.34 us
    all_to_all x1, starting transfers between devices, exchange(): lax.all_to_all(rows, 'ep', split_axis=0, concat_axis=0, axis_index_groups...  4.86 us
    pallas_call x1, Pallas kernels, local(): pl.pallas_call(expert_kernel, out_shape=jax.ShapeDtypeStruct(ROW_TILES, B...  2.26 us
  transfers between devices with their start and end apart: 1, of which 1 were waited for; matrix products, arithmetic and copies ran while one was open for 0% of the time, Pallas kernels for 17%

profile of v6, /device:TPU:1, one launch (start us, length us, event | category | flops | bytes accessed | tf_op | source)
XLA Modules:
  0.0 65.2 jit_solution(12912289108054682819)
XLA Ops:
  0.6 9.4 %front.1 = (bf16[48,16,128]{2,1,0:T(8,128)(2,1)S(1)}, bf16[256,16,128]{2,1,0:T(8,128)(2,1)S(1)}, f32[48,512]{1,0:T(8,128)S(1)}, f32[48,512]{1,0:T(8,128)S(1)}, s...) custom-call(s32[1,48]{1,0:T(1,128)} %bitcast.11, f32[1,128]{1,0:T(1,128)} %constant.2.clone.inv_hbm, ...), custom_call_target="tpu_custom_call" | custom-call | tf_op jit(solution)/shard_map/front/pallas_call | solution.py:416
  10.0 0.0 copy-start
  10.0 0.0 copy-start.1
  10.1 29.5 %all_to_all.10.in_ref = bf16[256,16,128]{2,1,0:T(8,128)(2,1)S(1)} all-to-all(bf16[256,16,128]{2,1,0:T(8,128)(2,1)S(1)} %get-tuple-element.12), channel_id=1, replica_groups={{21,53,85,117,29,61,93,125,5,37,69,101,13,45,77,109,23,55,87,119,31,63,..., dimensions={0} | all-to-all | bytes 2097152 | tf_op jit(solution)/shard_map/all_to_all | solution.py:498
  39.5 0.0 copy-done
  39.5 0.0 copy-done.1
  39.5 2.3 %expert.1 = bf16[256,16,128]{2,1,0:T(8,128)(2,1)} custom-call(bf16[256,16,128]{2,1,0:T(8,128)(2,1)S(1)} %all_to_all.10.in_ref, bf16[1,2048,256]{2,1,0:T(8,128)(2,1)S(1)} %copy-done, bf16[1,2048,256]{2,1,0:T(8,128)(2,1)S(1)} %copy-done.1, bf16[1,256,2048]{2,1,0:T(8,128)(2,1)S(1)} %get-tuple-element.13.wd_ref), custom_call_target="tpu_custom_call" | custom-call | flops 800000000 | bytes 4000000 | tf_op jit(solution)/shard_map/expert/pallas_call | solution.py:507
  41.8 4.9 %all-to-all-start.1 = ((bf16[256,16,128]{2,1,0:T(8,128)(2,1)}), bf16[256,16,128]{2,1,0:T(8,128)(2,1)S(1)}, u32[]{:S(2)}, u32[]{:S(2)}) async-start(bf16[256,16,128]{2,1,0:T(8,128)(2,1)} %expert.1), calls=%async_computation.1 | async-start | bytes 2097152 | tf_op jit(solution)/shard_map/all_to_all | solution.py:498
  46.7 11.4 %state_update.1 = f32[48,8,64,64]{3,2,1,0:T(8,128)} custom-call(f32[8]{0:T(128)} %decay.1, f32[48,8,64,64]{3,2,1,0:T(8,128)} %state_ref.1, f32[48,512]{1,0:T(8,128)S(1)} %get-tuple-element.14.k_ref, f32[48,512]{1,0:T(8,128)S(1)} %get-tuple-element.15.v_ref), custom_call_target="tpu_custom_call" | custom-call | flops 1000000000 | bytes 26000000 | tf_op jit(solution)/shard_map/state_update/pallas_call | solution.py:479
  58.0 6.3 %all-to-all-done.1.back_ref = bf16[256,16,128]{2,1,0:T(8,128)(2,1)S(1)} async-done(((bf16[256,16,128]{2,1,0:T(8,128)(2,1)}), bf16[256,16,128]{2,1,0:T(8,128)(2,1)S(1)}, u32[]{:S(2)}, u32[]{:S(2)}) %all-to-all-start.1) | async-done | bytes 1048608 | tf_op jit(solution)/shard_map/all_to_all | solution.py:498
  64.4 0.8 %combine.1 = bf16[48,2048]{1,0:T(8,128)(2,1)} custom-call(s32[2,48]{1,0:T(2,128)S(4)} %get-tuple-element.9.slot, f32[2,48]{1,0:T(2,128)S(4)} %get-tuple-element.10.weight, bf16[48,16,128]{2,1,0:T(8,128)(2,1)S(1)} %get-tuple-element.11.mixed_ref, bf16[256,16,128]{2,1,0:T(8,128)(2,1)S(1)} %all-to-all-done.1.back_ref), custom_call_target="tpu_custom_call" | custom-call | tf_op jit(solution)/shard_map/combine/pallas_call | solution.py:529
Async XLA Ops:
  10.0 29.5 %copy-start = (bf16[1,2048,256]{2,1,0:T(8,128)(2,1)S(1)}, bf16[1,2048,256]{2,1,0:T(8,128)(2,1)}, u32[]{:S(2)}) copy-start(bf16[1,2048,256]{2,1,0:T(8,128)(2,1)} %wg_ref.1) | copy-start | bytes 3145732
  10.0 29.5 %copy-start.1 = (bf16[1,2048,256]{2,1,0:T(8,128)(2,1)S(1)}, bf16[1,2048,256]{2,1,0:T(8,128)(2,1)}, u32[]{:S(2)}) copy-start(bf16[1,2048,256]{2,1,0:T(8,128)(2,1)} %wu_ref.1) | copy-start | bytes 3145732
  41.8 22.6 %all-to-all-start.1 = ((bf16[256,16,128]{2,1,0:T(8,128)(2,1)}), bf16[256,16,128]{2,1,0:T(8,128)(2,1)S(1)}, u32[]{:S(2)}, u32[]{:S(2)}) async-start(bf16[256,16,128]{2,1,0:T(8,128)(2,1)} %expert.1), calls=%async_computation.1 | async-start | bytes 2097152 | tf_op jit(solution)/shard_map/all_to_all | solution.py:498

commit v7 on v6

--- a/solution.py
+++ b/solution.py
@@ -38,11 +38,11 @@
 
 def out_place(group, inner):
     inner = inner ^ SHIFT
-    return group + (inner // 8) * 4 + (inner // 2 % 4) * 16 + (inner % 2) * 64
+    return group + (inner >> 3) * 4 + (inner >> 1 & 3) * 16 + (inner & 1) * 64
 
 
 def back_place(group, inner):
-    return group + (inner // 2 % 4) * 4 + (inner // 8) * 16 + (inner % 2) * 64
+    return group + (inner >> 1 & 3) * 4 + (inner >> 3) * 16 + (inner & 1) * 64
 
 
 def lane_iota(shape):

time: 65.4 us -> 64.9 us (level)
  transfers between devices with their start and end apart: 1 -> 1, of which waited for: 1 -> 1; matrix products, arithmetic and copies ran while one was open for 0% -> 0% of each run, Pallas kernels for 17% -> 18%
where the time goes in v7:
time: 64.9 us; the launch traced here: 64.6 us
  blocking collectives  29.5 us (45%)
  Pallas kernels  23.3 us (36%)
  waiting for transfers between devices  6.33 us (10%)
  starting transfers between devices  4.85 us (7%)
  between operations  0.68 us (1%)
    all_to_all x1, blocking collectives, exchange(): lax.all_to_all(rows, 'ep', split_axis=0, concat_axis=0, axis_index_groups...  29.5 us
    pallas_call x1, Pallas kernels, local(): pl.pallas_call(state_kernel, grid=(CHUNKS,), out_shape=jax.ShapeDtypeStru...  11.4 us
    pallas_call x1, Pallas kernels, local(): pl.pallas_call(front_kernel, out_shape=[pltpu.VMEM((ROWS, TILES, LANES),...  8.85 us
    all_to_all x1, waiting for transfers between devices, exchange(): lax.all_to_all(rows, 'ep', split_axis=0, concat_axis=0, axis_index_groups...  6.33 us
    all_to_all x1, starting transfers between devices, exchange(): lax.all_to_all(rows, 'ep', split_axis=0, concat_axis=0, axis_index_groups...  4.85 us
    pallas_call x1, Pallas kernels, local(): pl.pallas_call(expert_kernel, out_shape=jax.ShapeDtypeStruct(ROW_TILES, B...  2.27 us
  transfers between devices with their start and end apart: 1, of which 1 were waited for; matrix products, arithmetic and copies ran while one was open for 0% of the time, Pallas kernels for 18%

profile of v7, /device:TPU:1, one launch (start us, length us, event | category | flops | bytes accessed | tf_op | source)
XLA Modules:
  0.0 64.6 jit_solution(17383998498302701275)
XLA Ops:
  0.6 8.8 %front.1 = (bf16[48,16,128]{2,1,0:T(8,128)(2,1)S(1)}, bf16[256,16,128]{2,1,0:T(8,128)(2,1)S(1)}, f32[48,512]{1,0:T(8,128)S(1)}, f32[48,512]{1,0:T(8,128)S(1)}, s...) custom-call(s32[1,48]{1,0:T(1,128)} %bitcast.11, f32[1,128]{1,0:T(1,128)} %constant.2.clone.inv_hbm, ...), custom_call_target="tpu_custom_call" | custom-call | tf_op jit(solution)/shard_map/front/pallas_call | solution.py:416
  9.5 0.0 copy-start
  9.5 0.0 copy-start.1
  9.5 29.5 %all_to_all.10.in_ref = bf16[256,16,128]{2,1,0:T(8,128)(2,1)S(1)} all-to-all(bf16[256,16,128]{2,1,0:T(8,128)(2,1)S(1)} %get-tuple-element.12), channel_id=1, replica_groups={{21,53,85,117,29,61,93,125,5,37,69,101,13,45,77,109,23,55,87,119,31,63,..., dimensions={0} | all-to-all | bytes 2097152 | tf_op jit(solution)/shard_map/all_to_all | solution.py:498
  39.0 0.0 copy-done
  39.0 0.0 copy-done.1
  39.0 2.3 %expert.1 = bf16[256,16,128]{2,1,0:T(8,128)(2,1)} custom-call(bf16[256,16,128]{2,1,0:T(8,128)(2,1)S(1)} %all_to_all.10.in_ref, bf16[1,2048,256]{2,1,0:T(8,128)(2,1)S(1)} %copy-done, bf16[1,2048,256]{2,1,0:T(8,128)(2,1)S(1)} %copy-done.1, bf16[1,256,2048]{2,1,0:T(8,128)(2,1)S(1)} %get-tuple-element.13.wd_ref), custom_call_target="tpu_custom_call" | custom-call | flops 800000000 | bytes 4000000 | tf_op jit(solution)/shard_map/expert/pallas_call | solution.py:507
  41.3 4.9 %all-to-all-start.1 = ((bf16[256,16,128]{2,1,0:T(8,128)(2,1)}), bf16[256,16,128]{2,1,0:T(8,128)(2,1)S(1)}, u32[]{:S(2)}, u32[]{:S(2)}) async-start(bf16[256,16,128]{2,1,0:T(8,128)(2,1)} %expert.1), calls=%async_computation.1 | async-start | bytes 2097152 | tf_op jit(solution)/shard_map/all_to_all | solution.py:498
  46.1 11.4 %state_update.1 = f32[48,8,64,64]{3,2,1,0:T(8,128)} custom-call(f32[8]{0:T(128)} %decay.1, f32[48,8,64,64]{3,2,1,0:T(8,128)} %state_ref.1, f32[48,512]{1,0:T(8,128)S(1)} %get-tuple-element.14.k_ref, f32[48,512]{1,0:T(8,128)S(1)} %get-tuple-element.15.v_ref), custom_call_target="tpu_custom_call" | custom-call | flops 1000000000 | bytes 26000000 | tf_op jit(solution)/shard_map/state_update/pallas_call | solution.py:479
  57.5 6.3 %all-to-all-done.1.back_ref = bf16[256,16,128]{2,1,0:T(8,128)(2,1)S(1)} async-done(((bf16[256,16,128]{2,1,0:T(8,128)(2,1)}), bf16[256,16,128]{2,1,0:T(8,128)(2,1)S(1)}, u32[]{:S(2)}, u32[]{:S(2)}) %all-to-all-start.1) | async-done | bytes 1048608 | tf_op jit(solution)/shard_map/all_to_all | solution.py:498
  63.8 0.8 %combine.1 = bf16[48,2048]{1,0:T(8,128)(2,1)} custom-call(s32[2,48]{1,0:T(2,128)S(4)} %get-tuple-element.9.slot, f32[2,48]{1,0:T(2,128)S(4)} %get-tuple-element.10.weight, bf16[48,16,128]{2,1,0:T(8,128)(2,1)S(1)} %get-tuple-element.11.mixed_ref, bf16[256,16,128]{2,1,0:T(8,128)(2,1)S(1)} %all-to-all-done.1.back_ref), custom_call_target="tpu_custom_call" | custom-call | tf_op jit(solution)/shard_map/combine/pallas_call | solution.py:529
Async XLA Ops:
  9.5 29.5 %copy-start = (bf16[1,2048,256]{2,1,0:T(8,128)(2,1)S(1)}, bf16[1,2048,256]{2,1,0:T(8,128)(2,1)}, u32[]{:S(2)}) copy-start(bf16[1,2048,256]{2,1,0:T(8,128)(2,1)} %wg_ref.1) | copy-start | bytes 3145732
  9.5 29.5 %copy-start.1 = (bf16[1,2048,256]{2,1,0:T(8,128)(2,1)S(1)}, bf16[1,2048,256]{2,1,0:T(8,128)(2,1)}, u32[]{:S(2)}) copy-start(bf16[1,2048,256]{2,1,0:T(8,128)(2,1)} %wu_ref.1) | copy-start | bytes 3145732
  41.3 22.6 %all-to-all-start.1 = ((bf16[256,16,128]{2,1,0:T(8,128)(2,1)}), bf16[256,16,128]{2,1,0:T(8,128)(2,1)S(1)}, u32[]{:S(2)}, u32[]{:S(2)}) async-start(bf16[256,16,128]{2,1,0:T(8,128)(2,1)} %expert.1), calls=%async_computation.1 | async-start | bytes 2097152 | tf_op jit(solution)/shard_map/all_to_all | solution.py:498

commit v8 on v7

--- a/solution.py
+++ b/solution.py
@@ -19,6 +19,8 @@
 TILES = D // LANES
 GROUP = 8
 CHUNKS = ROWS // GROUP
+PIECE = 4
+PIECES = ROWS // PIECE
 STEP = 20
 PART = 16
 COPIES = 4
@@ -162,7 +164,7 @@
     down_copy = pltpu.make_async_copy(down_hbm, down_ref, w_sem.at[5])
 
     def state_copy(i):
-        rows = pl.ds(i * GROUP, GROUP)
+        rows = pl.ds(i * PIECE, PIECE)
         return pltpu.make_async_copy(state_hbm.at[rows], st.at[rows], st_sem.at[i])
 
     for copy in small:
@@ -171,7 +173,8 @@
         copy.start()
     for copy in small:
         copy.wait()
-    state_copy(0).start()
+    for i in range(2):
+        state_copy(i).start()
 
     x = tok[...].astype(F32)
     scale = lax.rsqrt(jnp.mean(x * x, axis=-1, keepdims=True) + EPS)
@@ -210,11 +213,11 @@
         return jnp.dot(normed, w4[i], preferred_element_type=F32).astype(BF16).astype(F32)
 
     q = project(0)
-    for i in range(1, 3):
+    for i in range(2, 6):
         state_copy(i).start()
     q = rope(q, cosine, sine)
     k = project(1)
-    for i in range(3, CHUNKS):
+    for i in range(6, PIECES):
         state_copy(i).start()
     wo_copy.start()
     k = rope(k, cosine, sine) * (HD**-0.5)
@@ -250,11 +253,11 @@
 
     def chunk(i, carry):
         state_copy(i).wait()
-        for b in range(GROUP):
-            read(i * GROUP + b)
+        for b in range(PIECE):
+            read(i * PIECE + b)
         return carry
 
-    lax.fori_loop(0, CHUNKS, chunk, 0)
+    lax.fori_loop(0, PIECES, chunk, 0)
 
     def head_rows(h):
         return part[pl.ds(h, ROWS, stride=HEADS + 1), :]
@@ -447,7 +450,7 @@
             pltpu.VMEM((ROWS, LANES), F32),
             pltpu.SemaphoreType.DMA((10,)),
             pltpu.SemaphoreType.DMA((6,)),
-            pltpu.SemaphoreType.DMA((CHUNKS,)),
+            pltpu.SemaphoreType.DMA((PIECES,)),
         ],
         compiler_params=pltpu.CompilerParams(vmem_limit_bytes=32 * 2**20),
         name="front",

time: 64.9 us -> 65 us (level)
  no operation moved by 1% of the time
where the time goes in v8:
time: 65 us; the launch traced here: 64.7 us
  blocking collectives  29.5 us (45%)
  Pallas kernels  23.4 us (36%)
  waiting for transfers between devices  6.34 us (10%)
  starting transfers between devices  4.85 us (7%)
  between operations  0.68 us (1%)
    all_to_all x1, blocking collectives, exchange(): lax.all_to_all(rows, 'ep', split_axis=0, concat_axis=0, axis_index_groups...  29.5 us
    pallas_call x1, Pallas kernels, local(): pl.pallas_call(state_kernel, grid=(CHUNKS,), out_shape=jax.ShapeDtypeStru...  11.4 us
    pallas_call x1, Pallas kernels, local(): pl.pallas_call(front_kernel, out_shape=[pltpu.VMEM((ROWS, TILES, LANES),...  8.94 us
    all_to_all x1, waiting for transfers between devices, exchange(): lax.all_to_all(rows, 'ep', split_axis=0, concat_axis=0, axis_index_groups...  6.34 us
    all_to_all x1, starting transfers between devices, exchange(): lax.all_to_all(rows, 'ep', split_axis=0, concat_axis=0, axis_index_groups...  4.85 us
    pallas_call x1, Pallas kernels, local(): pl.pallas_call(expert_kernel, out_shape=jax.ShapeDtypeStruct(ROW_TILES, B...  2.27 us
  transfers between devices with their start and end apart: 1, of which 1 were waited for; matrix products, arithmetic and copies ran while one was open for 0% of the time, Pallas kernels for 18%

profile of v8, /device:TPU:1, one launch (start us, length us, event | category | flops | bytes accessed | tf_op | source)
XLA Modules:
  0.0 64.7 jit_solution(5359879542943933305)
XLA Ops:
  0.6 8.9 %front.1 = (bf16[48,16,128]{2,1,0:T(8,128)(2,1)S(1)}, bf16[256,16,128]{2,1,0:T(8,128)(2,1)S(1)}, f32[48,512]{1,0:T(8,128)S(1)}, f32[48,512]{1,0:T(8,128)S(1)}, s...) custom-call(s32[1,48]{1,0:T(1,128)} %bitcast.11, f32[1,128]{1,0:T(1,128)} %constant.2.clone.inv_hbm, ...), custom_call_target="tpu_custom_call" | custom-call | tf_op jit(solution)/shard_map/front/pallas_call | solution.py:419
  9.6 0.0 copy-start
  9.6 0.0 copy-start.1
  9.6 29.5 %all_to_all.10.in_ref = bf16[256,16,128]{2,1,0:T(8,128)(2,1)S(1)} all-to-all(bf16[256,16,128]{2,1,0:T(8,128)(2,1)S(1)} %get-tuple-element.12), channel_id=1, replica_groups={{21,53,85,117,29,61,93,125,5,37,69,101,13,45,77,109,23,55,87,119,31,63,..., dimensions={0} | all-to-all | bytes 2097152 | tf_op jit(solution)/shard_map/all_to_all | solution.py:501
  39.1 0.0 copy-done
  39.1 0.0 copy-done.1
  39.1 2.3 %expert.1 = bf16[256,16,128]{2,1,0:T(8,128)(2,1)} custom-call(bf16[256,16,128]{2,1,0:T(8,128)(2,1)S(1)} %all_to_all.10.in_ref, bf16[1,2048,256]{2,1,0:T(8,128)(2,1)S(1)} %copy-done, bf16[1,2048,256]{2,1,0:T(8,128)(2,1)S(1)} %copy-done.1, bf16[1,256,2048]{2,1,0:T(8,128)(2,1)S(1)} %get-tuple-element.13.wd_ref), custom_call_target="tpu_custom_call" | custom-call | flops 800000000 | bytes 4000000 | tf_op jit(solution)/shard_map/expert/pallas_call | solution.py:510
  41.3 4.9 %all-to-all-start.1 = ((bf16[256,16,128]{2,1,0:T(8,128)(2,1)}), bf16[256,16,128]{2,1,0:T(8,128)(2,1)S(1)}, u32[]{:S(2)}, u32[]{:S(2)}) async-start(bf16[256,16,128]{2,1,0:T(8,128)(2,1)} %expert.1), calls=%async_computation.1 | async-start | bytes 2097152 | tf_op jit(solution)/shard_map/all_to_all | solution.py:501
  46.2 11.4 %state_update.1 = f32[48,8,64,64]{3,2,1,0:T(8,128)} custom-call(f32[8]{0:T(128)} %decay.1, f32[48,8,64,64]{3,2,1,0:T(8,128)} %state_ref.1, f32[48,512]{1,0:T(8,128)S(1)} %get-tuple-element.14.k_ref, f32[48,512]{1,0:T(8,128)S(1)} %get-tuple-element.15.v_ref), custom_call_target="tpu_custom_call" | custom-call | flops 1000000000 | bytes 26000000 | tf_op jit(solution)/shard_map/state_update/pallas_call | solution.py:482
  57.6 6.3 %all-to-all-done.1.back_ref = bf16[256,16,128]{2,1,0:T(8,128)(2,1)S(1)} async-done(((bf16[256,16,128]{2,1,0:T(8,128)(2,1)}), bf16[256,16,128]{2,1,0:T(8,128)(2,1)S(1)}, u32[]{:S(2)}, u32[]{:S(2)}) %all-to-all-start.1) | async-done | bytes 1048608 | tf_op jit(solution)/shard_map/all_to_all | solution.py:501
  63.9 0.8 %combine.1 = bf16[48,2048]{1,0:T(8,128)(2,1)} custom-call(s32[2,48]{1,0:T(2,128)S(4)} %get-tuple-element.9.slot, f32[2,48]{1,0:T(2,128)S(4)} %get-tuple-element.10.weight, bf16[48,16,128]{2,1,0:T(8,128)(2,1)S(1)} %get-tuple-element.11.mixed_ref, bf16[256,16,128]{2,1,0:T(8,128)(2,1)S(1)} %all-to-all-done.1.back_ref), custom_call_target="tpu_custom_call" | custom-call | tf_op jit(solution)/shard_map/combine/pallas_call | solution.py:532
Async XLA Ops:
  9.6 29.5 %copy-start = (bf16[1,2048,256]{2,1,0:T(8,128)(2,1)S(1)}, bf16[1,2048,256]{2,1,0:T(8,128)(2,1)}, u32[]{:S(2)}) copy-start(bf16[1,2048,256]{2,1,0:T(8,128)(2,1)} %wg_ref.1) | copy-start | bytes 3145732
  9.6 29.5 %copy-start.1 = (bf16[1,2048,256]{2,1,0:T(8,128)(2,1)S(1)}, bf16[1,2048,256]{2,1,0:T(8,128)(2,1)}, u32[]{:S(2)}) copy-start(bf16[1,2048,256]{2,1,0:T(8,128)(2,1)} %wu_ref.1) | copy-start | bytes 3145732
  41.3 22.6 %all-to-all-start.1 = ((bf16[256,16,128]{2,1,0:T(8,128)(2,1)}), bf16[256,16,128]{2,1,0:T(8,128)(2,1)S(1)}, u32[]{:S(2)}, u32[]{:S(2)}) async-start(bf16[256,16,128]{2,1,0:T(8,128)(2,1)} %expert.1), calls=%async_computation.1 | async-start | bytes 2097152 | tf_op jit(solution)/shard_map/all_to_all | solution.py:501
